TPU v7x, 512 devices: a whole 4x8x8 slice. The times are simulated.
512 devices in a mesh: ep: 128 (over z, y, core), tp: 4 (over x).
Axes of the slice: x: 4, y: 8, z: 8, core: 2. Of those that a mesh axis runs over, the one named last changes fastest.
Arguments:
- tokens: bfloat16 [2048, 1024], P('ep', 'tp'), may hold values from -12 to 12
- input_window: bfloat16 [2048, 3, 512], P('ep', None, 'tp'), may hold values from -6 to 6
- write_window: bfloat16 [2048, 3, 256], P('ep', None, 'tp'), may hold values from -6 to 6
- read_window: bfloat16 [2048, 3, 256], P('ep', None, 'tp'), may hold values from -6 to 6
- ssm_state: float32 [2048, 8, 64, 64], P('ep', 'tp'), may hold values from -6 to 6
- norm_gain: bfloat16 [1024], replicated, may hold values from 0.099609375 to 1.8984375
- proj_gate: bfloat16 [1024, 512], P(None, 'tp'), may hold values from -0.1875 to 0.1875
- proj_input: bfloat16 [1024, 512], P(None, 'tp'), may hold values from -0.1875 to 0.1875
- proj_write: bfloat16 [1024, 256], P(None, 'tp'), may hold values from -0.1875 to 0.1875
- proj_read: bfloat16 [1024, 256], P(None, 'tp'), may hold values from -0.1875 to 0.1875
- proj_step: bfloat16 [1024, 8], replicated, may hold values from -0.1875 to 0.1875
- taps_input: bfloat16 [4, 512], P(None, 'tp'), may hold values from -3 to 3
- taps_write: bfloat16 [4, 256], P(None, 'tp'), may hold values from -3 to 3
- taps_read: bfloat16 [4, 256], P(None, 'tp'), may hold values from -3 to 3
- step_bias: float32 [8], replicated, may hold values from -2.5 to 0.5
- decay_rate: float32 [8], replicated, may hold values from 0.02 to 2
- skip_gain: float32 [8], replicated, may hold values from 0.1 to 1.9
- out_gain: bfloat16 [512], P('tp'), may hold values from 0.099609375 to 1.8984375
- proj_out: bfloat16 [512, 1024], P('tp'), may hold values from -0.25 to 0.25
- ffn_gain: bfloat16 [1024], replicated, may hold values from 0.099609375 to 1.8984375
- expert_ids: int32 [2048, 6], P('ep'), may hold values from 0 to 127, all different within a row; in each aligned block of 16 rows (0 to 15, 16 to 31, ...) at most 2 rows name the same one
- expert_weights: float32 [2048, 6], P('ep'), may hold values from 0.05 to 1
- expert_gate: bfloat16 [128, 1024, 512], P('ep', None, 'tp'), may hold values from -0.1875 to 0.1875
- expert_up: bfloat16 [128, 1024, 512], P('ep', None, 'tp'), may hold values from -0.1875 to 0.1875
- expert_down: bfloat16 [128, 512, 1024], P('ep', 'tp'), may hold values from -0.25 to 0.25
- dense_gate: bfloat16 [1024, 1024], P(None, 'tp'), may hold values from -0.1875 to 0.1875
- dense_up: bfloat16 [1024, 1024], P(None, 'tp'), may hold values from -0.1875 to 0.1875
- dense_down: bfloat16 [1024, 1024], P(None, 'tp'), may hold values from -0.5 to 0.5
- branch_gate: bfloat16 [1024], replicated, may hold values from -0.1875 to 0.1875
Outputs:
- new_hidden: bfloat16 [2048, 1024], P('ep', 'tp')
- new_state: float32 [2048, 8, 64, 64], P('ep', 'tp')
- new_input_window: bfloat16 [2048, 3, 512], P('ep', None, 'tp')
- new_write_window: bfloat16 [2048, 3, 256], P('ep', None, 'tp')
- new_read_window: bfloat16 [2048, 3, 256], P('ep', None, 'tp')
Inputs may be any that keep to these rules, and one draw needn't show every extreme that they name: `expert_ids`: each row names 6 different experts. Among the 16 rows of one index of ep no expert is named more than 2 times, and in some aligned block an expert is named exactly 2 times.
All inputs are finite; a program needn't handle non-finite values.
Results may differ from a plain program's by a relative error of at most 0.018.
Values may be sent and summed in bfloat16 or wider, within the bound.
No kernel may reach another device: no remote copies, remote signals or barrier semaphores. Data moves between devices by JAX's collectives and lax.ppermute only.
A program may use at most 64 MiB of HBM per device.

v0:
```python
import jax
import jax.numpy as jnp
from jax import lax
from jax.sharding import PartitionSpec as P

HEADS = 8
HEAD_DIM = 64
STATE = 64
BC_GROUPS = 4


EPS = 1e-06


def laid_out(pieces, dim):
    dims = list(pieces.shape[1:])
    dims[dim] *= pieces.shape[0]
    return jnp.moveaxis(pieces, 0, dim).reshape(dims)


def from_everyone(value, axis):
    devices = lax.axis_size(axis)
    return lax.all_to_all(
        jnp.broadcast_to(value[None], (devices, *value.shape)), axis, 0, 0, tiled=True
    )


def gather_directly(value, axis, dim):
    return laid_out(from_everyone(value, axis), dim)


def over_copies(value, axis):
    everything = from_everyone(value, axis)
    return jnp.sum(everything.astype(jnp.float32), axis=0)


def cut_along(value, dim, devices):
    before, after = (value.shape[:dim], value.shape[dim + 1 :])
    return jnp.moveaxis(value.reshape(*before, devices, -1, *after), dim, 0)


def summed_on_arrival(value, axis, dim):
    pieces = cut_along(value, dim, lax.axis_size(axis))
    arrived = lax.all_to_all(pieces, axis, split_axis=0, concat_axis=0, tiled=True)
    return arrived.astype(jnp.float32).sum(axis=0)


def short_conv(window, newest, taps):
    stacked = jnp.concatenate([window, newest[:, None, :]], axis=1)
    mixed = jnp.sum(stacked.astype(jnp.float32) * taps.astype(jnp.float32)[None], axis=1)
    return (jax.nn.silu(mixed), stacked[:, 1:, :])


def norm_rows(values, gain):
    widened = values.astype(jnp.float32)
    scale = lax.rsqrt(jnp.mean(widened * widened, axis=-1, keepdims=True) + EPS)
    return widened * scale * gain.astype(jnp.float32)


def local(
    tokens,
    input_window,
    write_window,
    read_window,
    ssm_state,
    norm_gain,
    proj_gate,
    proj_input,
    proj_write,
    proj_read,
    proj_step,
    taps_input,
    taps_write,
    taps_read,
    step_bias,
    decay_rate,
    skip_gain,
    out_gain,
    proj_out,
    ffn_gain,
    expert_ids,
    expert_weights,
    expert_gate,
    expert_up,
    expert_down,
    dense_gate,
    dense_up,
    dense_down,
    branch_gate,
):
    tp_rank = lax.axis_index("tp")
    ep_count = lax.axis_size("ep")
    row_count = tokens.shape[0]
    width = norm_gain.shape[0]
    quarter = tokens.shape[1]
    col_start = tp_rank * quarter
    full_tokens = gather_directly(tokens, "tp", 1)
    normed = norm_rows(full_tokens, norm_gain).astype(jnp.bfloat16)
    heads_dev = proj_gate.shape[1] // HEAD_DIM
    head_start = tp_rank * heads_dev
    per_group = HEADS // BC_GROUPS
    groups_dev = heads_dev // per_group
    gate_rows = jnp.dot(normed, proj_gate, preferred_element_type=jnp.float32).astype(jnp.bfloat16)
    input_rows = jnp.dot(normed, proj_input, preferred_element_type=jnp.float32).astype(
        jnp.bfloat16
    )
    write_rows = jnp.dot(normed, proj_write, preferred_element_type=jnp.float32).astype(
        jnp.bfloat16
    )
    read_rows = jnp.dot(normed, proj_read, preferred_element_type=jnp.float32).astype(jnp.bfloat16)
    step_all = jnp.dot(normed, proj_step, preferred_element_type=jnp.float32)
    step_raw = lax.dynamic_slice_in_dim(step_all, head_start, heads_dev, 1)
    input_conv, new_input_window = short_conv(input_window, input_rows, taps_input)
    write_conv, new_write_window = short_conv(write_window, write_rows, taps_write)
    read_conv, new_read_window = short_conv(read_window, read_rows, taps_read)
    bias_part = lax.dynamic_slice_in_dim(step_bias, head_start, heads_dev, 0)
    rate_part = lax.dynamic_slice_in_dim(decay_rate, head_start, heads_dev, 0)
    skip_part = lax.dynamic_slice_in_dim(skip_gain, head_start, heads_dev, 0)
    step_size = jax.nn.softplus(step_raw + bias_part)
    decay = jnp.exp(-step_size * rate_part)
    heads_input = input_conv.reshape(row_count, heads_dev, HEAD_DIM)
    write_heads = jnp.repeat(write_conv.reshape(row_count, groups_dev, STATE), per_group, axis=1)
    read_heads = jnp.repeat(read_conv.reshape(row_count, groups_dev, STATE), per_group, axis=1)
    new_state = (
        decay[:, :, None, None] * ssm_state
        + (step_size[:, :, None] * heads_input)[:, :, :, None] * write_heads[:, :, None, :]
    )
    readout = jnp.einsum("bhpn,bhn->bhp", new_state, read_heads)
    readout = readout + skip_part[None, :, None] * heads_input
    gated = readout.reshape(row_count, heads_dev * HEAD_DIM) * jax.nn.silu(
        gate_rows.astype(jnp.float32)
    )
    grouped = gated.reshape(row_count, groups_dev, -1)
    grouped = grouped * lax.rsqrt(jnp.mean(grouped * grouped, axis=-1, keepdims=True) + EPS)
    mixer_rows = (
        grouped.reshape(row_count, heads_dev * HEAD_DIM) * out_gain.astype(jnp.float32)
    ).astype(jnp.bfloat16)
    partial_value = jnp.dot(mixer_rows, proj_out, preferred_element_type=jnp.float32)
    mixed = over_copies(partial_value.astype(jnp.bfloat16), "tp").astype(jnp.float32)
    hidden_full = (full_tokens.astype(jnp.float32) + mixed).astype(jnp.bfloat16)
    normed_ffn = norm_rows(hidden_full, ffn_gain).astype(jnp.bfloat16)
    hidden_part = lax.dynamic_slice_in_dim(hidden_full, col_start, quarter, 1)
    local_experts = expert_gate.shape[0]
    expert_total = local_experts * ep_count
    top_count = expert_ids.shape[1]
    capacity = min(
        row_count, max(2, (3 * row_count * top_count + 2 * expert_total - 1) // (2 * expert_total))
    )
    slot_total = expert_total * capacity
    flat_ids = expert_ids.reshape(-1)
    hits = (flat_ids[:, None] == jnp.arange(expert_total, dtype=jnp.int32)[None, :]).astype(
        jnp.int32
    )
    before = jnp.cumsum(hits, axis=0) - hits
    place = jnp.sum(before * hits, axis=1)
    slots = (flat_ids * capacity + place).reshape(row_count, top_count)
    matches = slots[:, :, None] == jnp.arange(slot_total, dtype=jnp.int32)[None, None, :]
    chosen = jnp.any(matches, axis=1).astype(jnp.bfloat16)
    outgoing = jnp.einsum("rs,rd->sd", chosen, normed_ffn, preferred_element_type=jnp.float32)
    outgoing = outgoing.astype(jnp.bfloat16).reshape(expert_total, capacity, width)
    arrived = lax.all_to_all(outgoing, "ep", split_axis=0, concat_axis=0, tiled=True)
    item_count = arrived.shape[1]
    grouped_in = arrived.reshape(-1, local_experts, item_count, width)
    gate_part = jnp.einsum(
        "secd,edf->secf", grouped_in, expert_gate, preferred_element_type=jnp.float32
    )
    up_part = jnp.einsum(
        "secd,edf->secf", grouped_in, expert_up, preferred_element_type=jnp.float32
    )
    hidden = (jax.nn.silu(gate_part) * up_part).astype(jnp.bfloat16)
    partial_out = jnp.einsum(
        "secf,efd->secd", hidden, expert_down, preferred_element_type=jnp.float32
    )
    summed = summed_on_arrival(
        partial_out.reshape(-1, item_count, width).astype(jnp.bfloat16), "tp", 2
    )
    processed = summed.astype(jnp.bfloat16)
    returned = lax.all_to_all(processed, "ep", split_axis=0, concat_axis=0, tiled=True)
    weights_on = jnp.sum(jnp.where(matches, expert_weights[:, :, None], 0.0), axis=1)
    expert_sum = jnp.dot(weights_on, returned.reshape(slot_total, quarter).astype(jnp.float32))
    dense_hidden = (
        jax.nn.silu(jnp.dot(normed_ffn, dense_gate, preferred_element_type=jnp.float32))
        * jnp.dot(normed_ffn, dense_up, preferred_element_type=jnp.float32)
    ).astype(jnp.bfloat16)
    dense_partial = lax.dot_general(
        dense_hidden, dense_down, (((1,), (1,)), ((), ())), preferred_element_type=jnp.float32
    )
    dense_sum = summed_on_arrival(dense_partial.astype(jnp.bfloat16), "tp", 1)
    branch = jax.nn.sigmoid(jnp.dot(normed_ffn, branch_gate, preferred_element_type=jnp.float32))
    new_hidden = (
        hidden_part.astype(jnp.float32) + expert_sum + branch[:, None] * dense_sum
    ).astype(jnp.bfloat16)
    return (new_hidden, new_state, new_input_window, new_write_window, new_read_window)


def solution(mesh):
    in_specs = (
        P("ep", "tp"),
        P("ep", None, "tp"),
        P("ep", None, "tp"),
        P("ep", None, "tp"),
        P("ep", "tp", None, None),
        P(),
        P(None, "tp"),
        P(None, "tp"),
        P(None, "tp"),
        P(None, "tp"),
        P(),
        P(None, "tp"),
        P(None, "tp"),
        P(None, "tp"),
        P(),
        P(),
        P(),
        P("tp"),
        P("tp", None),
        P(),
        P("ep", None),
        P("ep", None),
        P("ep", None, "tp"),
        P("ep", None, "tp"),
        P("ep", "tp", None),
        P(None, "tp"),
        P(None, "tp"),
        P(None, "tp"),
        P(),
    )
    out_specs = (
        P("ep", "tp"),
        P("ep", "tp", None, None),
        P("ep", None, "tp"),
        P("ep", None, "tp"),
        P("ep", None, "tp"),
    )
    return jax.shard_map(local, mesh=mesh, in_specs=in_specs, out_specs=out_specs, check_vma=False)
```

profile of v0, /device:TPU:1, one launch (start us, length us, event | category | flops | bytes accessed | tf_op | source)
XLA Modules:
  0.0 117.8 jit_solution(8965787524016152022)
XLA Ops:
  0.7 1.4 %broadcast_in_dim.18 = bf16[4,16,256]{2,1,0:T(8,128)(2,1)} broadcast(bf16[16,256]{1,0:T(8,128)(2,1)} %param.29), dimensions={1,2} | broadcast | bytes 40960 | tf_op jit(solution)/shard_map/broadcast_in_dim | solution.py:24
  2.1 4.8 %all-to-all-start = ((bf16[4,16,256]{2,1,0:T(8,128)(2,1)}), bf16[4,16,256]{2,1,0:T(8,128)(2,1)S(1)}, u32[]{:S(2)}, u32[]{:S(2)}) async-start(bf16[4,16,256]{2,1,0:T(8,128)(2,1)} %broadcast_in_dim.18), calls=%async_computation | async-start | bytes 65536 | tf_op jit(solution)/shard_map/all_to_all | solution.py:23
  6.9 0.8 copy.100
  7.7 0.1 eq.28
  7.8 0.1 fusion.33
  7.9 0.1 reduce_window_sum.11
  8.0 0.2 select_reduce_fusion.1
  8.3 0.1 copy.101
  8.3 0.7 multiply_add_fusion.2
  9.1 0.7 convert_element_type.132
  9.7 0.7 convert_element_type.139
  10.4 0.7 dynamic_slice.17
  11.1 0.7 dynamic_slice.16
  11.9 0.7 convert_element_type.136
  12.6 0.7 convert_element_type.142
  13.2 0.7 dynamic_slice.18
  14.0 0.7 convert_element_type.145
  14.6 0.7 convert_element_type.155
  15.3 0.1 fusion.31
  15.5 1.1 fusion.9
  16.6 0.7 multiply_reduce_fusion.2
  17.3 0.8 fusion.48
  18.2 0.1 multiply_exponential_fusion
  18.3 0.1 copy.99
  18.4 1.1 fusion.8
  19.6 0.1 copy.98
  19.7 0.1 fusion.10
  19.8 0.6 copy-done.11
  20.4 0.1 broadcast_multiply_fusion
  20.5 0.4 multiply_add_fusion
  21.0 0.4 fusion.49
  21.4 0.1 multiply_add_fusion.1
  21.5 0.6 copy-done.5
  22.1 0.3 multiply_reduce_fusion.4
  22.4 0.2 convolution_convert_fusion.2
  22.6 0.7 broadcast_in_dim.22
  23.3 4.2 %all-to-all-start.1 = ((bf16[4,16,1024]{2,1,0:T(8,128)(2,1)}), bf16[4,16,1024]{2,1,0:T(8,128)(2,1)S(1)}, u32[]{:S(2)}, u32[]{:S(2)}) async-start(bf16[4,16,1024]{2,1,0:T(8,128)(2,1)} %broadcast_in_dim.22), calls=%async_computation.1 | async-start | bytes 262144 | tf_op jit(solution)/shard_map/all_to_all | solution.py:23
  27.6 4.7 %all-to-all-done.1 = bf16[4,16,1024]{2,1,0:T(8,128)(2,1)S(1)} async-done(((bf16[4,16,1024]{2,1,0:T(8,128)(2,1)}), bf16[4,16,1024]{2,1,0:T(8,128)(2,1)S(1)}, u32[]{:S(2)}, u32[]{:S(2)}) %all-to-all-start.1) | async-done | bytes 131104 | tf_op jit(solution)/shard_map/all_to_all | solution.py:23
  32.4 0.1 multiply_reduce_fusion
  32.5 0.4 convolution_convert_fusion.1
  32.9 1.0 reshape.130
  33.9 19.7 %all-to-all-start.2 = ((bf16[128,2,1024]{2,1,0:T(2,128)(2,1)}), bf16[128,2,1024]{2,1,0:T(2,128)(2,1)S(1)}, u32[]{:S(2)}, u32[]{:S(2)}) async-start(bf16[128,2,1024]{2,1,0:T(2,128)(2,1)} %reshape.130), calls=%async_computation.2 | async-start | bytes 1048576 | tf_op jit(solution)/shard_map/all_to_all | solution.py:161
  53.7 0.6 copy-done.13
  54.3 0.1 select_reduce_fusion
  54.4 0.6 fusion.39
  55.0 19.1 %all-to-all-done.2 = bf16[128,2,1024]{2,1,0:T(2,128)(2,1)S(1)} async-done(((bf16[128,2,1024]{2,1,0:T(2,128)(2,1)}), bf16[128,2,1024]{2,1,0:T(2,128)(2,1)S(1)}, u32[]{:S(2)}, u32[]{:S(2)}) %all-to-all-start.2) | async-done | bytes 524320 | tf_op jit(solution)/shard_map/all_to_all | solution.py:161
  74.2 0.3 convolution_bitcast_fusion.1
  74.5 0.5 fusion
  75.0 0.4 convert_element_type.163
  75.4 0.9 copy.125
  76.3 3.6 %all-to-all-start.3 = ((bf16[4,128,2,256]{3,1,2,0:T(8,128)(2,1)}), bf16[4,128,2,256]{3,1,2,0:T(8,128)(2,1)S(1)}, u32[]{:S(2)}, u32[]{:S(2)}) async-start(bf16[4,128,2,256]{3,1,2,0:T(8,128)(2,1)} %bitcast.113), calls=%async_computation.3 | async-start | bytes 1048576 | tf_op jit(solution)/shard_map/all_to_all | solution.py:44
  79.9 0.2 fusion.47
  80.1 0.8 copy-done.4
  80.9 0.5 convolution_convert_fusion.3
  81.4 0.6 copy.126
  82.1 7.6 %all-to-all-done.3 = bf16[4,128,2,256]{3,1,2,0:T(8,128)(2,1)S(1)} async-done(((bf16[4,128,2,256]{3,1,2,0:T(8,128)(2,1)}), bf16[4,128,2,256]{3,1,2,0:T(8,128)(2,1)S(1)}, u32[]{:S(2)}, u32[]{:S(2)}) %all-to-all-start.3) | async-done | bytes 524320 | tf_op jit(solution)/shard_map/all_to_all | solution.py:44
  89.7 3.3 %all-to-all-start.5 = ((bf16[4,16,256]{2,1,0:T(8,128)(2,1)}), bf16[4,16,256]{2,1,0:T(8,128)(2,1)S(1)}, u32[]{:S(2)}, u32[]{:S(2)}) async-start(bf16[4,16,256]{2,1,0:T(8,128)(2,1)} %bitcast.115), calls=%async_computation.5 | async-start | bytes 65536 | tf_op jit(solution)/shard_map/all_to_all | solution.py:44
  92.9 0.6 fusion.41
  93.6 0.8 copy.107
  94.4 2.8 %all-to-all-done.5 = bf16[4,16,256]{2,1,0:T(8,128)(2,1)S(1)} async-done(((bf16[4,16,256]{2,1,0:T(8,128)(2,1)}), bf16[4,16,256]{2,1,0:T(8,128)(2,1)S(1)}, u32[]{:S(2)}, u32[]{:S(2)}) %all-to-all-start.5) | async-done | bytes 32800 | tf_op jit(solution)/shard_map/all_to_all | solution.py:44
  97.2 6.9 %all-to-all-start.4 = ((bf16[128,2,256]{2,1,0:T(2,128)(2,1)}), bf16[128,2,256]{2,1,0:T(2,128)(2,1)S(1)}, u32[]{:S(2)}, u32[]{:S(2)}) async-start(bf16[128,2,256]{2,1,0:T(2,128)(2,1)} %copy.107), calls=%async_computation.4 | async-start | bytes 262144 | tf_op jit(solution)/shard_map/all_to_all | solution.py:178
  104.1 0.2 fusion.14
  104.3 12.6 %all-to-all-done.4 = bf16[128,2,256]{2,1,0:T(2,128)(2,1)S(1)} async-done(((bf16[128,2,256]{2,1,0:T(2,128)(2,1)}), bf16[128,2,256]{2,1,0:T(2,128)(2,1)S(1)}, u32[]{:S(2)}, u32[]{:S(2)}) %all-to-all-start.4) | async-done | bytes 131104 | tf_op jit(solution)/shard_map/all_to_all | solution.py:178
  117.0 0.8 fusion.5
  (50 shorter events, 0.7 us)
Async XLA Ops:
  0.6 79.5 %copy-start = (bf16[1024,256]{1,0:T(8,128)(2,1)S(1)}, bf16[1024,256]{1,0:T(8,128)(2,1)}, u32[]{:S(2)}) copy-start(bf16[1024,256]{1,0:T(8,128)(2,1)} %param.56) | copy-start | bytes 1572868
  0.6 19.9 %copy-start.2 = (f32[16,2,64,64]{3,2,1,0:T(8,128)S(1)}, f32[16,2,64,64]{3,2,1,0:T(8,128)}, u32[]{:S(2)}) copy-start(f32[16,2,64,64]{3,2,1,0:T(8,128)} %param.33) | copy-start | bytes 1572868
  2.1 13.2 %all-to-all-start = ((bf16[4,16,256]{2,1,0:T(8,128)(2,1)}), bf16[4,16,256]{2,1,0:T(8,128)(2,1)S(1)}, u32[]{:S(2)}, u32[]{:S(2)}) async-start(bf16[4,16,256]{2,1,0:T(8,128)(2,1)} %broadcast_in_dim.18), calls=%async_computation | async-start | bytes 65536 | tf_op jit(solution)/shard_map/all_to_all | solution.py:23
  18.4 1.2 copy-start.12
  18.4 1.3 %copy-start.9 = (bf16[1024,64]{0,1:T(8,128)(2,1)S(1)}, bf16[1024,64]{0,1:T(8,128)(2,1)}, u32[]{:S(2)}) copy-start(bf16[1024,64]{0,1:T(8,128)(2,1)} %param.38) | copy-start | bytes 393220
  19.7 0.7 copy-start.11
  20.9 2.3 %copy-start.1 = (f32[16,2,64,64]{3,2,1,0:T(8,128)}, f32[16,2,64,64]{3,2,1,0:T(8,128)S(1)}, u32[]{:S(2)}) copy-start(f32[16,2,64,64]{3,2,1,0:T(8,128)S(1)} %multiply_add_fusion) | copy-start | bytes 1572868
  21.0 1.2 copy-start.5
  21.4 1.1 copy-start.6
  23.3 9.1 %all-to-all-start.1 = ((bf16[4,16,1024]{2,1,0:T(8,128)(2,1)}), bf16[4,16,1024]{2,1,0:T(8,128)(2,1)S(1)}, u32[]{:S(2)}, u32[]{:S(2)}) async-start(bf16[4,16,1024]{2,1,0:T(8,128)(2,1)} %broadcast_in_dim.22), calls=%async_computation.1 | async-start | bytes 262144 | tf_op jit(solution)/shard_map/all_to_all | solution.py:23
  33.9 19.7 %copy-start.14 = (bf16[1024]{0:T(1024)(128)(2,1)S(1)}, bf16[1024]{0:T(1024)(128)(2,1)}, u32[]{:S(2)}) copy-start(bf16[1024]{0:T(1024)(128)(2,1)} %param.57) | copy-start | bytes 6148
  33.9 40.3 %copy-start.15 = (bf16[1,1024,128]{2,1,0:T(8,128)(2,1)S(1)}, bf16[1,1024,128]{2,1,0:T(8,128)(2,1)}, u32[]{:S(2)}) copy-start(bf16[1,1024,128]{2,1,0:T(8,128)(2,1)} %param.51) | copy-start | bytes 786436
  33.9 40.3 %all-to-all-start.2 = ((bf16[128,2,1024]{2,1,0:T(2,128)(2,1)}), bf16[128,2,1024]{2,1,0:T(2,128)(2,1)S(1)}, u32[]{:S(2)}, u32[]{:S(2)}) async-start(bf16[128,2,1024]{2,1,0:T(2,128)(2,1)} %reshape.130), calls=%async_computation.2 | async-start | bytes 1048576 | tf_op jit(solution)/shard_map/all_to_all | solution.py:161
  53.6 0.7 copy-start.13
  53.6 0.8 copy-start.10
  55.0 19.5 %copy-start.7 = (bf16[1,128,1024]{2,1,0:T(8,128)(2,1)S(1)}, bf16[1,128,1024]{2,1,0:T(8,128)(2,1)}, u32[]{:S(2)}) copy-start(bf16[1,128,1024]{2,1,0:T(8,128)(2,1)} %param.53) | copy-start | bytes 786436
  55.0 19.5 %copy-start.8 = (bf16[1,1024,128]{2,1,0:T(8,128)(2,1)S(1)}, bf16[1,1024,128]{2,1,0:T(8,128)(2,1)}, u32[]{:S(2)}) copy-start(bf16[1,1024,128]{2,1,0:T(8,128)(2,1)} %param.52) | copy-start | bytes 786436
  76.3 3.6 %copy-start.3 = (bf16[1024,256]{1,0:T(8,128)(2,1)S(1)}, bf16[1024,256]{1,0:T(8,128)(2,1)}, u32[]{:S(2)}) copy-start(bf16[1024,256]{1,0:T(8,128)(2,1)} %param.54) | copy-start | bytes 1572868
  76.3 13.4 %all-to-all-start.3 = ((bf16[4,128,2,256]{3,1,2,0:T(8,128)(2,1)}), bf16[4,128,2,256]{3,1,2,0:T(8,128)(2,1)S(1)}, u32[]{:S(2)}, u32[]{:S(2)}) async-start(bf16[4,128,2,256]{3,1,2,0:T(8,128)(2,1)} %bitcast.113), calls=%async_computation.3 | async-start | bytes 1048576 | tf_op jit(solution)/shard_map/all_to_all | solution.py:44
  79.9 1.0 copy-start.4
  89.7 7.5 %all-to-all-start.5 = ((bf16[4,16,256]{2,1,0:T(8,128)(2,1)}), bf16[4,16,256]{2,1,0:T(8,128)(2,1)S(1)}, u32[]{:S(2)}, u32[]{:S(2)}) async-start(bf16[4,16,256]{2,1,0:T(8,128)(2,1)} %bitcast.115), calls=%async_computation.5 | async-start | bytes 65536 | tf_op jit(solution)/shard_map/all_to_all | solution.py:44
  97.2 19.7 %all-to-all-start.4 = ((bf16[128,2,256]{2,1,0:T(2,128)(2,1)}), bf16[128,2,256]{2,1,0:T(2,128)(2,1)S(1)}, u32[]{:S(2)}, u32[]{:S(2)}) async-start(bf16[128,2,256]{2,1,0:T(2,128)(2,1)} %copy.107), calls=%async_computation.4 | async-start | bytes 262144 | tf_op jit(solution)/shard_map/all_to_all | solution.py:178
where the time goes:
time: 119 us; the launch traced here: 118 us
  waiting for transfers between devices  46.9 us (39%)
  starting transfers between devices  42.6 us (36%)
  local copies, waits for them, and re-layouts  12 us (10%)
  other arithmetic  8.46 us (7%)
  matrix products  6.86 us (6%)
    all_to_all x1, starting transfers between devices, local(): lax.all_to_all(outgoing, 'ep', split_axis=0, concat_axis=0, tiled=True)  19.7 us
    all_to_all x1, waiting for transfers between devices, local(): lax.all_to_all(outgoing, 'ep', split_axis=0, concat_axis=0, tiled=True)  19.1 us
    all_to_all x1, waiting for transfers between devices, local(): lax.all_to_all(processed, 'ep', split_axis=0, concat_axis=0, tiled=True)  12.6 us
    all_to_all x2, waiting for transfers between devices, summed_on_arrival(): lax.all_to_all(pieces, axis, split_axis=0, concat_axis=0, tiled=True)  10.4 us
    all_to_all x2, starting transfers between devices, from_everyone(): lax.all_to_all(jnp.broadcast_to(value[None], (devices, *value.shape)), ax...  9.07 us
    all_to_all x1, starting transfers between devices, local(): lax.all_to_all(processed, 'ep', split_axis=0, concat_axis=0, tiled=True)  6.92 us
    all_to_all x2, starting transfers between devices, summed_on_arrival(): lax.all_to_all(pieces, axis, split_axis=0, concat_axis=0, tiled=True)  6.86 us
    all_to_all x2, waiting for transfers between devices, from_everyone(): lax.all_to_all(jnp.broadcast_to(value[None], (devices, *value.shape)), ax...  4.74 us
  transfers between devices with their start and end apart: 6, of which 5 were waited for; matrix products, arithmetic and copies ran while one was open for 10% of the time, Pallas kernels for 0%

commit v1 on v0

v1 whole, which is shorter than its diff:
```python
import functools

import jax
import jax.numpy as jnp
from jax import lax
from jax.experimental import pallas as pl
from jax.experimental.pallas import tpu as pltpu
from jax.sharding import PartitionSpec as P

HEADS = 8
HEAD_DIM = 64
STATE = 64
EPS = 1e-06
F32 = jnp.float32
BF16 = jnp.bfloat16

HBM = pl.BlockSpec(memory_space=pltpu.HBM)
VMEM = pl.BlockSpec(memory_space=pltpu.VMEM)
SMEM = pl.BlockSpec(memory_space=pltpu.SMEM)
INTERPRET = False
LIMIT = 16 * 1024 * 1024


def call(body, outs, specs, name, scratch=(), out_spec=VMEM):
    return pl.pallas_call(
        body,
        out_shape=outs,
        in_specs=specs,
        out_specs=jax.tree.map(lambda _: out_spec, outs),
        scratch_shapes=scratch,
        compiler_params=pltpu.CompilerParams(vmem_limit_bytes=LIMIT),
        name=name,
        interpret=INTERPRET,
    )


def kept(value):
    return pltpu.with_memory_space_constraint(value, pltpu.HBM)


def sds(shape, dtype):
    return jax.ShapeDtypeStruct(shape, dtype)


def nt(a, b):
    return lax.dot_general(a, b, (((1,), (1,)), ((), ())), preferred_element_type=F32)


def nn(a, b):
    return jnp.dot(a, b, preferred_element_type=F32)


def silu(v):
    return v / (1.0 + jnp.exp(-v))


def softplus(v):
    return jnp.maximum(v, 0.0) + jnp.log1p(jnp.exp(-jnp.abs(v)))


def spread_body(tokens, out, sems):
    copies = [
        pltpu.make_async_copy(tokens, out.at[j], sems.at[j]) for j in range(out.shape[0])
    ]
    for copy in copies:
        copy.start()
    for copy in copies:
        copy.wait()


def zeros_and_ones(shape, test):
    across = lax.broadcasted_iota(jnp.int32, shape, 1)
    down = lax.broadcasted_iota(jnp.int32, shape, 0)
    return test(down, across).astype(F32).astype(BF16)


def route(rank, ids, weights, select, combine):
    tops, rows = ids.shape
    experts = combine.shape[1] // 8
    pieces = select.shape[0] // experts
    expert = lax.broadcasted_iota(jnp.int32, (experts, rows), 0)
    hits = jnp.zeros((experts, rows), F32)
    amount = jnp.zeros((experts, rows), F32)
    for k in range(tops):
        same = expert == ids[k : k + 1, :]
        hits = jnp.where(same, 1.0, hits)
        amount = jnp.where(same, weights[k : k + 1, :], amount)
    earlier = zeros_and_ones((rows, rows), lambda d, a: d < a)
    place = nn(hits.astype(BF16), earlier)
    mine = jnp.bitwise_and(rank[0], 1).astype(F32)
    chosen = jnp.where(place == mine, hits, 0.0).astype(BF16)
    down = zeros_and_ones((experts * pieces, experts), lambda d, a: d // pieces == a)
    across = zeros_and_ones((rows, rows * pieces), lambda d, a: a // pieces == d)
    wide = nn(nn(down, chosen).astype(BF16), across)
    matched = zeros_and_ones(wide.shape, lambda d, a: d % pieces == a % pieces)
    select[...] = wide.astype(BF16) * matched
    twice = zeros_and_ones((experts, experts * 2), lambda d, a: a // 2 == d)
    halves = lax.broadcasted_iota(jnp.int32, (rows, experts * 2), 1) % 2
    for s in range(2):
        part = jnp.where(place == float(s), amount, 0.0).T
        high = part.astype(BF16)
        low = (part - high.astype(F32)).astype(BF16)
        for p, piece in enumerate((high, low)):
            both = nn(piece, twice)
            for h in range(2):
                rows_at = (2 * p + h) * rows
                kept = jnp.where(halves == h, both, 0.0).astype(BF16)
                for t in (s, s + 2):
                    combine[
                        rows_at : rows_at + rows, t * 2 * experts : (t + 1) * 2 * experts
                    ] = kept


STAGED = 14


def prepare_body(*refs):
    rank, ids, weights, bias, rate, skip, gate, up, down = refs[:9]
    sources = refs[9 : 9 + STAGED]
    select, combine, lanes, packed = refs[9 + STAGED : 13 + STAGED]
    targets = refs[13 + STAGED : 13 + 2 * STAGED]
    ids_here, weights_here, bias_here, rate_here, skip_here, sems = refs[13 + 2 * STAGED :]
    width, block = gate.shape
    pairs = [
        (ids, ids_here),
        (weights, weights_here),
        (bias, bias_here),
        (rate, rate_here),
        (skip, skip_here),
    ]
    pairs += list(zip(sources, targets))
    pairs += [(gate, packed.at[0:width]), (up, packed.at[width : 2 * width])]
    for j in range(width // block):
        first = 2 * width + j * block
        pairs.append((down.at[:, j * block : (j + 1) * block], packed.at[first : first + block]))
    copies = [pltpu.make_async_copy(a, b, sems.at[k]) for k, (a, b) in enumerate(pairs)]
    for copy in copies:
        copy.start()
    for copy in copies[:5]:
        copy.wait()
    route(rank, ids_here, weights_here, select, combine)
    inner = lanes.shape[1]
    heads = inner // HEAD_DIM
    lane_head = lax.broadcasted_iota(jnp.int32, (1, inner), 1) // HEAD_DIM
    for k, table in enumerate((bias_here, rate_here, skip_here)):
        line = jnp.zeros((1, inner), F32)
        for h in range(heads):
            line = jnp.where(lane_head == h, table[rank[0] * heads + h], line)
        lanes[k : k + 1, :] = line
    for copy in copies[5:]:
        copy.wait()


def conv(window, newest, taps, out_window):
    taken = taps[...].astype(F32)
    total = newest.astype(F32) * taken[3:4]
    for k in range(3):
        total += window[k].astype(F32) * taken[k : k + 1]
    out_window[0] = window[1]
    out_window[1] = window[2]
    out_window[2] = newest
    return silu(total)


def mixer_body(
    rank,
    lanes,
    arrived,
    norm_gain,
    proj_gate,
    proj_input,
    proj_write,
    proj_read,
    proj_step,
    taps_input,
    taps_write,
    taps_read,
    input_window,
    write_window,
    read_window,
    state,
    out_gain,
    proj_out,
    partial,
    new_state,
    new_input_window,
    new_write_window,
    new_read_window,
):
    rows = arrived.shape[1]
    x = jnp.concatenate([arrived[j] for j in range(arrived.shape[0])], axis=1).astype(F32)
    scale = lax.rsqrt(jnp.mean(x * x, axis=-1, keepdims=True) + EPS)
    normed = (x * scale * norm_gain[...].astype(F32)[None, :]).astype(BF16)
    gate_rows = nn(normed, proj_gate[...]).astype(BF16)
    input_rows = nn(normed, proj_input[...]).astype(BF16)
    write_rows = nt(normed, proj_write[...]).astype(BF16)
    read_rows = nt(normed, proj_read[...]).astype(BF16)
    step_all = nt(normed, proj_step[...])
    input_conv = conv(input_window, input_rows, taps_input, new_input_window)
    write_conv = conv(write_window, write_rows, taps_write, new_write_window)
    read_conv = conv(read_window, read_rows, taps_read, new_read_window)
    inner = input_conv.shape[1]
    heads = inner // HEAD_DIM
    lane_head = lax.broadcasted_iota(jnp.int32, (rows, inner), 1) // HEAD_DIM
    column = lax.broadcasted_iota(jnp.int32, step_all.shape, 1)
    raw = jnp.zeros((rows, inner), F32)
    for h in range(heads):
        mine = column == rank[0] * heads + h
        raw = jnp.where(
            lane_head == h, jnp.sum(jnp.where(mine, step_all, 0.0), axis=1, keepdims=True), raw
        )
    step = softplus(raw + lanes[0:1, :])
    decay = jnp.exp(-step * lanes[1:2, :])
    scaled_t = (step * input_conv).T
    decay_t = decay.T
    lane = lax.broadcasted_iota(jnp.int32, (inner, rows), 1)
    readout_t = jnp.zeros((inner, rows), F32)
    for b in range(rows):
        fresh = (
            decay_t[:, b : b + 1] * state[b] + scaled_t[:, b : b + 1] * write_conv[b : b + 1, :]
        )
        new_state[b] = fresh
        seen = jnp.sum(fresh * read_conv[b : b + 1, :], axis=1, keepdims=True)
        readout_t = jnp.where(lane == b, seen, readout_t)
    readout = readout_t.T + lanes[2:3, :] * input_conv
    gated = readout * silu(gate_rows.astype(F32))
    gated = gated * lax.rsqrt(jnp.mean(gated * gated, axis=-1, keepdims=True) + EPS)
    mixer_rows = (gated * out_gain[...].astype(F32)[None, :]).astype(BF16)
    mixed = nn(mixer_rows, proj_out[...]).astype(BF16)
    for j in range(partial.shape[0]):
        partial[j] = mixed


def hidden_body(
    rank, arrived, mixed_in, ffn_gain, select, outgoing, normed_out, hidden_part, folded
):
    count, rows, quarter = arrived.shape
    x = jnp.concatenate([arrived[j] for j in range(count)], axis=1).astype(F32)
    mixed = mixed_in[0].astype(F32)
    for j in range(1, count):
        mixed += mixed_in[j].astype(F32)
    hidden = (x + mixed).astype(BF16)
    wide = hidden.astype(F32)
    scale = lax.rsqrt(jnp.mean(wide * wide, axis=-1, keepdims=True) + EPS)
    normed_wide = wide * scale * ffn_gain[...].astype(F32)[None, :]
    normed_out[...] = normed_wide.astype(BF16)
    pieces = folded.shape[0] // rows
    for j in range(pieces):
        folded[pl.ds(j, rows, stride=pieces), :] = normed_wide[:, j * 128 : (j + 1) * 128]
    outgoing[...] = nn(select[...], folded[...].astype(BF16)).astype(BF16)
    part = wide[:, 0:quarter]
    for j in range(1, count):
        part = jnp.where(rank[0] == j, wide[:, j * quarter : (j + 1) * quarter], part)
    hidden_part[...] = part.astype(BF16)


def dense_body(
    rank, normed_in, gate, up, down, branch_gate, out0, out1, out2, out3, branch, pieces
):
    normed = normed_in[...]
    hidden = (silu(nn(normed, gate[...])) * nn(normed, up[...])).astype(BF16)
    total = nt(hidden, down[...]).astype(BF16)
    quarter = out0.shape[1]
    for j in range(pieces.shape[0]):
        pieces[j] = total[:, j * quarter : (j + 1) * quarter]
    for k, out in enumerate((out0, out1, out2, out3)):
        out[...] = pieces[jnp.bitwise_and(rank[0] + k, 3)]
    level = jnp.sum(
        normed.astype(F32) * branch_gate[...].astype(F32)[None, :], axis=-1, keepdims=True
    )
    branch[...] = jnp.broadcast_to(jax.nn.sigmoid(level), branch.shape)


def expert_body(items, gate, up, down, other, out, unfolded, fold):
    width, block = gate.shape
    pieces = width // 128
    count = items.shape[0] // pieces
    unfolded[...] = items[...].astype(F32)
    x = jnp.concatenate(
        [unfolded[pl.ds(j, count, stride=pieces), :].astype(BF16) for j in range(pieces)], axis=1
    )
    act = (silu(nn(x, gate[...])) * nn(x, up[...])).astype(BF16)
    act_other = (silu(nn(x, other[0:width])) * nn(x, other[width : 2 * width])).astype(BF16)
    total = nn(act, down[...])
    for j in range(pieces):
        first = 2 * width + j * block
        piece = total[:, j * block : (j + 1) * block] + nn(act_other, other[first : first + block])
        fold[pl.ds(j // 2 * 2 * count + j % 2, count, stride=2), :] = piece
    out[...] = fold[...].astype(BF16)


def final_body(returned, combine, dense0, dense1, dense2, dense3, branch, hidden_part, out):
    total = hidden_part[...].astype(F32)
    rows = total.shape[0]
    dense = dense0[...].astype(F32)
    for piece in (dense1, dense2, dense3):
        dense += piece[...].astype(F32)
    sums = nn(combine[...], returned[...])
    sums = sums[0 : 2 * rows] + sums[2 * rows :]
    total += jnp.concatenate([sums[0:rows], sums[rows:]], axis=1)
    total += branch[:, 0:1] * dense
    out[...] = total.astype(BF16)


def local(
    tokens,
    input_window,
    write_window,
    read_window,
    ssm_state,
    norm_gain,
    proj_gate,
    proj_input,
    proj_write,
    proj_read,
    proj_step,
    taps_input,
    taps_write,
    taps_read,
    step_bias,
    decay_rate,
    skip_gain,
    out_gain,
    proj_out,
    ffn_gain,
    expert_ids,
    expert_weights,
    expert_gate,
    expert_up,
    expert_down,
    dense_gate,
    dense_up,
    dense_down,
    branch_gate,
):
    tps = lax.axis_size("tp")
    eps = lax.axis_size("ep")
    rank = lax.axis_index("tp").astype(jnp.int32).reshape(1)
    rows, quarter = tokens.shape
    width = quarter * tps
    inner = proj_gate.shape[1]
    latent = proj_write.shape[1]
    heads = ssm_state.shape[1]
    block = expert_gate.shape[2]

    pieces = width // 128

    spread = call(
        spread_body,
        sds((tps, rows, quarter), BF16),
        [HBM],
        "spread",
        [pltpu.SemaphoreType.DMA((tps,))],
        HBM,
    )(kept(tokens))
    with jax.named_scope("gather"):
        arrived = lax.all_to_all(spread, "tp", 0, 0, tiled=True)

    staged = (
        norm_gain,
        proj_gate,
        proj_input,
        proj_write.T,
        proj_read.T,
        proj_step.T,
        taps_input,
        taps_write,
        taps_read,
        input_window.transpose(1, 0, 2),
        write_window.transpose(1, 0, 2),
        read_window.transpose(1, 0, 2),
        ssm_state.reshape(rows, inner, STATE),
        out_gain,
    )
    ids, weights = expert_ids.T, expert_weights.T
    select, combine, lanes, packed, *staged = call(
        prepare_body,
        (
            sds((eps * pieces, rows * pieces), BF16),
            sds((4 * rows, 2 * tps * eps), BF16),
            sds((8, inner), F32),
            sds((3 * width, block), BF16),
        )
        + tuple(sds(v.shape, v.dtype) for v in staged),
        [SMEM] + [HBM] * (8 + STAGED),
        "prepare",
        [
            pltpu.VMEM(ids.shape, ids.dtype),
            pltpu.VMEM(weights.shape, F32),
            pltpu.SMEM(step_bias.shape, F32),
            pltpu.SMEM(step_bias.shape, F32),
            pltpu.SMEM(step_bias.shape, F32),
            pltpu.SemaphoreType.DMA((7 + pieces + STAGED,)),
        ],
    )(
        rank,
        *map(
            kept,
            (
                ids,
                weights,
                step_bias,
                decay_rate,
                skip_gain,
                expert_gate[0],
                expert_up[0],
                expert_down[0],
                *staged,
            ),
        ),
    )

    partial, new_state, new_input, new_write, new_read = call(
        mixer_body,
        (
            sds((tps, rows, width), BF16),
            sds((rows, inner, STATE), F32),
            sds((3, rows, inner), BF16),
            sds((3, rows, latent), BF16),
            sds((3, rows, latent), BF16),
        ),
        [SMEM] + [VMEM] * 17,
        "mixer",
    )(rank, lanes, arrived, *staged, proj_out)
    with jax.named_scope("mix"):
        mixed_in = lax.all_to_all(partial, "tp", 0, 0, tiled=True)
    packed, mixed_in = lax.optimization_barrier((packed, mixed_in))
    with jax.named_scope("swap"):
        other = lax.ppermute(packed, "tp", [(t, t ^ 1) for t in range(tps)])

    outgoing, normed_ffn, hidden_part = call(
        hidden_body,
        (
            sds((eps * pieces, 128), BF16),
            sds((rows, width), BF16),
            sds((rows, quarter), BF16),
        ),
        [SMEM] + [VMEM] * 4,
        "hidden",
        [pltpu.VMEM((rows * pieces, 128), F32)],
    )(rank, arrived, mixed_in, ffn_gain, select)
    items = lax.all_to_all(outgoing.reshape(eps, pieces, 128), "ep", 0, 0, tiled=True)

    dense_out = call(
        dense_body,
        (sds((rows, quarter), BF16),) * tps + (sds((rows, 128), F32),),
        [SMEM] + [VMEM] * 5,
        "dense",
        [pltpu.VMEM((tps, rows, quarter), BF16)],
    )(rank, normed_ffn, dense_gate, dense_up, dense_down, branch_gate)
    branch = dense_out[tps]
    dense_in = [dense_out[0]]
    for k in range(1, tps):
        with jax.named_scope("dense_swap"):
            turn = [(t, (t + k) % tps) for t in range(tps)]
            dense_in.append(lax.ppermute(dense_out[k], "tp", turn))

    results = call(
        expert_body,
        sds((tps * eps * 2, 128), BF16),
        [VMEM] * 5,
        "experts",
        [pltpu.VMEM((eps * pieces, 128), F32), pltpu.VMEM((tps * eps * 2, 128), F32)],
    )(items.reshape(eps * pieces, 128), expert_gate[0], expert_up[0], expert_down[0], other)
    returned = lax.all_to_all(
        results.reshape(tps * eps, 2, 128), ("tp", "ep"), 0, 0, tiled=True
    ).reshape(tps * eps * 2, 128)

    new_hidden = call(final_body, sds((rows, quarter), BF16), [VMEM] * 8, "final")(
        returned, combine, *dense_in, branch, hidden_part
    )
    return (
        new_hidden,
        new_state.reshape(rows, heads, HEAD_DIM, STATE),
        new_input.transpose(1, 0, 2),
        new_write.transpose(1, 0, 2),
        new_read.transpose(1, 0, 2),
    )


def solution(mesh):
    in_specs = (
        P("ep", "tp"),
        P("ep", None, "tp"),
        P("ep", None, "tp"),
        P("ep", None, "tp"),
        P("ep", "tp", None, None),
        P(),
        P(None, "tp"),
        P(None, "tp"),
        P(None, "tp"),
        P(None, "tp"),
        P(),
        P(None, "tp"),
        P(None, "tp"),
        P(None, "tp"),
        P(),
        P(),
        P(),
        P("tp"),
        P("tp", None),
        P(),
        P("ep", None),
        P("ep", None),
        P("ep", None, "tp"),
        P("ep", None, "tp"),
        P("ep", "tp", None),
        P(None, "tp"),
        P(None, "tp"),
        P(None, "tp"),
        P(),
    )
    out_specs = (
        P("ep", "tp"),
        P("ep", "tp", None, None),
        P("ep", None, "tp"),
        P("ep", None, "tp"),
        P("ep", None, "tp"),
    )
    return jax.shard_map(local, mesh=mesh, in_specs=in_specs, out_specs=out_specs, check_vma=False)
```

time: 119 us -> 89 us (0.75)
  blocking collectives: 0 us -> 42.8 us
  waiting for transfers between devices: 46.9 us -> 8.13 us
  starting transfers between devices: 42.6 us -> 26.5 us
  local copies, waits for them, and re-layouts: 12 us -> 0.05 us
  Pallas kernels: 0 us -> 10.2 us
  other arithmetic: 8.46 us -> 0 us
  matrix products: 6.86 us -> 0 us
    all_to_all x0 -> x2, blocking collectives: none -> 42.8 us  [the longest x1 35.6 us: local(): lax.all_to_all(outgoing.reshape(eps, pieces, 128), 'ep', 0, 0, tiled=True)]
    all_to_all x6 -> x2, waiting for transfers between devices: 46.9 us -> 6.51 us  [the longest x1 4.19 us: local(): lax.all_to_all(results.reshape(tps * eps, 2, 128), ('tp', 'ep'), 0, 0, ti...]
    all_to_all x6 -> x2, starting transfers between devices: 42.6 us -> 13.5 us  [the longest x1 8.67 us: local(): lax.all_to_all(results.reshape(tps * eps, 2, 128), ('tp', 'ep'), 0, 0, ti...]
    ppermute x0 -> x4, starting transfers between devices: none -> 13 us  [the longest x3 10.7 us: local(): dense_in.append(lax.ppermute(dense_out[k], 'tp', turn))]
    pallas_call x0 -> x7, Pallas kernels: none -> 10.2 us  [the longest x1 3.19 us: local(): call(mixer_body, (sds((tps, rows, width), BF16), sds((rows, inner, STATE)...]
    dot_general x14 -> x0, matrix products: 6.86 us -> none  [the longest x1 1.15 us: local(): jnp.dot(normed, proj_input, preferred_element_type=jnp.float32)]
    convert_element_type x9 -> x0, other arithmetic: 4.24 us -> none  [the longest x3 2.04 us: short_conv(): taps.astype(jnp.float32)[None]]
    unnamed x34 -> x18, local copies, waits for them, and re-layouts: 3.48 us -> 0.05 us
  transfers between devices with their start and end apart: 6 -> 6, of which waited for: 5 -> 3; matrix products, arithmetic and copies ran while one was open for 10% -> 0% of each run, Pallas kernels for 0% -> 3%
where the time goes in v1:
time: 89 us; the launch traced here: 88.6 us
  blocking collectives  42.8 us (48%)
  starting transfers between devices  26.5 us (30%)
  Pallas kernels  10.2 us (11%)
  waiting for transfers between devices  8.13 us (9%)
    all_to_all x1, blocking collectives, local(): lax.all_to_all(outgoing.reshape(eps, pieces, 128), 'ep', 0, 0, tiled=True)  35.6 us
    ppermute x3, starting transfers between devices, local(): dense_in.append(lax.ppermute(dense_out[k], 'tp', turn))  10.7 us
    all_to_all x1, starting transfers between devices, local(): lax.all_to_all(results.reshape(tps * eps, 2, 128), ('tp', 'ep'), 0, 0, ti...  8.67 us
    all_to_all x1, blocking collectives, local(): mixed_in = lax.all_to_all(partial, 'tp', 0, 0, tiled=True)  7.2 us
    all_to_all x1, starting transfers between devices, local(): arrived = lax.all_to_all(spread, 'tp', 0, 0, tiled=True)  4.84 us
    all_to_all x1, waiting for transfers between devices, local(): lax.all_to_all(results.reshape(tps * eps, 2, 128), ('tp', 'ep'), 0, 0, ti...  4.19 us
    pallas_call x1, Pallas kernels, local(): call(mixer_body, (sds((tps, rows, width), BF16), sds((rows, inner, STATE)...  3.19 us
    all_to_all x1, waiting for transfers between devices, local(): arrived = lax.all_to_all(spread, 'tp', 0, 0, tiled=True)  2.32 us
  transfers between devices with their start and end apart: 6, of which 3 were waited for; matrix products, arithmetic and copies ran while one was open for 0% of the time, Pallas kernels for 3%

profile of v1, /device:TPU:1, one launch (start us, length us, event | category | flops | bytes accessed | tf_op | source)
XLA Modules:
  0.0 88.6 jit_solution(8667580234069694232)
XLA Ops:
  0.6 2.1 %spread.1 = bf16[4,16,256]{2,1,0:T(8,128)(2,1)} custom-call(bf16[16,256]{1,0:T(8,128)(2,1)} %tokens.1), custom_call_target="tpu_custom_call" | custom-call | tf_op jit(solution)/shard_map/spread/pallas_call | solution.py:348
  2.8 4.8 %all-to-all-start = ((bf16[4,16,256]{2,1,0:T(8,128)(2,1)}), bf16[4,16,256]{2,1,0:T(8,128)(2,1)S(1)}, u32[]{:S(2)}, u32[]{:S(2)}) async-start(bf16[4,16,256]{2,1,0:T(8,128)(2,1)} %spread.1), calls=%async_computation | async-start | bytes 65536 | tf_op jit(solution)/shard_map/gather/all_to_all | solution.py:357
  7.6 0.0 copy-start.6
  7.6 2.0 %prepare.1 = (bf16[1024,128]{1,0:T(8,128)(2,1)S(1)}, bf16[64,1024]{1,0:T(8,128)(2,1)S(1)}, f32[8,128]{1,0:T(8,128)S(1)}, bf16[3072,128]{1,0:T(8,128)(2,1)S(1)}, ...) custom-call(s32[1]{0:T(128)} %bitcast.refs_0_.rank, ...), custom_call_target="tpu_custom_call" | custom-call | tf_op jit(solution)/shard_map/prepare/pallas_call | solution.py:376
  9.6 2.3 %all-to-all-done.arrived = bf16[4,16,256]{2,1,0:T(8,128)(2,1)S(1)} async-done(((bf16[4,16,256]{2,1,0:T(8,128)(2,1)}), bf16[4,16,256]{2,1,0:T(8,128)(2,1)S(1)}, u32[]{:S(2)}, u32[]{:S(2)}) %all-to-all-start) | async-done | bytes 32800 | tf_op jit(solution)/shard_map/gather/all_to_all | solution.py:357
  11.9 0.0 copy-done.6
  11.9 3.2 %mixer.1 = (bf16[4,16,1024]{2,1,0:T(8,128)(2,1)S(1)}, f32[16,128,64]{2,1,0:T(8,128)}, bf16[3,16,128]{2,1,0:T(8,128)(2,1)}, bf16[3,16,64]{2,1,0:T(8,128)(2,1)}, bf16[3,16,64]{2,1,0:T(8,128)(2,1)}) custom-call(s32[1]{0:T(128)} %bitcast.refs_0_.rank, f32[8,128]{1,0:T(8,128)S(1)} %get-tuple-element.39.lanes, bf16[4,16,256]{2,1,0:T(8,128)(2,1)S(1)} %all-to-all-done.arrived, ...), custom_call_target="tpu_custom_call" | custom-call | tf_op jit(solution)/shard_map/mixer/pallas_call | solution.py:413
  15.1 7.2 %all_to_all.20.mixed_in = bf16[4,16,1024]{2,1,0:T(8,128)(2,1)S(1)} all-to-all(bf16[4,16,1024]{2,1,0:T(8,128)(2,1)S(1)} %get-tuple-element.54), channel_id=1, replica_groups=mesh['ep'=128,'tp'=4] {'tp'}, dimensions={0} | all-to-all | bytes 262144 | tf_op jit(solution)/shard_map/mix/all_to_all | solution.py:426
  22.3 0.0 copy-start.7
  22.3 2.3 %collective-permute-start = (bf16[3072,128]{1,0:T(8,128)(2,1)S(1)}, bf16[3072,128]{1,0:T(8,128)(2,1)S(1)}, u32[]{:S(2)}, u32[]{:S(2)}) collective-permute-start(bf16[3072,128]{1,0:T(8,128)(2,1)S(1)} %get-tuple-element.58), channel_id=1, source_target_pairs={{0,1},{1,0},{2,3},{3,2},{4,5},{5,4},{6,7},{7,6},{8,9},{9,8},{10,11... | collective-permute-start | bytes 2359304 | tf_op jit(solution)/shard_map/swap/ppermute | solution.py:429
  24.6 0.0 copy-done.7
  24.6 0.0 copy-start.2
  24.7 0.3 hidden.1
  25.0 0.0 copy-start
  25.0 0.0 copy-start.1
  25.0 35.6 %all_to_all.21 = bf16[128,8,128]{2,1,0:T(8,128)(2,1)S(1)} all-to-all(bf16[128,8,128]{2,1,0:T(8,128)(2,1)S(1)} %bitcast.29), channel_id=1, replica_groups=mesh['ep'=128,'tp'=4] {'ep'}, dimensions={0} | all-to-all | bytes 524288 | tf_op jit(solution)/shard_map/all_to_all | solution.py:442
  60.6 0.0 collective-permute-done.other
  60.6 0.0 copy-done.2
  60.6 0.0 copy-done
  60.6 0.0 copy-done.1
  60.7 0.0 copy-start.4
  60.7 0.0 copy-start.5
  60.7 1.4 %experts.1 = bf16[1024,128]{1,0:T(8,128)(2,1)} custom-call(bf16[1024,128]{1,0:T(8,128)(2,1)S(1)} %bitcast.28, bf16[1024,128]{1,0:T(8,128)(2,1)S(1)} %bitcast.23, bf16[1024,128]{1,0:T(8,128)(2,1)S(1)} %bitcast.25, bf16[128,1024]{1,0:T(8,128)(2,1)S(1)} %bitcast.27, bf16[3072,128]{1,0:T(8,128)(2,1)S(1)} %collective-permute-done.other), custom_call_target="tpu_custom_call" | custom-call | tf_op jit(solution)/shard_map/experts/pallas_call | solution.py:458
  62.1 0.0 copy-start.3
  62.1 0.0 copy-start.8
  62.1 8.7 %all-to-all-start.3 = ((bf16[512,2,128]{2,1,0:T(2,128)(2,1)}), bf16[512,2,128]{2,1,0:T(2,128)(2,1)S(1)}, u32[]{:S(2)}, u32[]{:S(2)}) async-start(bf16[512,2,128]{2,1,0:T(2,128)(2,1)} %bitcast.15), calls=%async_computation.3 | async-start | bytes 524288 | tf_op jit(solution)/shard_map/all_to_all | solution.py:465
  70.8 0.0 copy-done.4
  70.8 0.0 copy-done.5
  70.8 0.0 copy-done.3
  70.8 0.0 copy-done.8
  70.8 0.4 dense.1
  71.2 3.3 %collective-permute-start.1 = (bf16[16,256]{1,0:T(8,128)(2,1)S(1)}, bf16[16,256]{1,0:T(8,128)(2,1)S(1)}, u32[]{:S(2)}, u32[]{:S(2)}) collective-permute-start(bf16[16,256]{1,0:T(8,128)(2,1)S(1)} %get-tuple-element.62), channel_id=1, source_target_pairs={{0,1},{1,2},{2,3},{3,0},{4,5},{5,6},{6,7},{7,4},{8,9},{9,10},{10,1... | collective-permute-start | bytes 24584 | tf_op jit(solution)/shard_map/dense_swap/ppermute | solution.py:456
  74.5 4.3 %collective-permute-start.2 = (bf16[16,256]{1,0:T(8,128)(2,1)S(1)}, bf16[16,256]{1,0:T(8,128)(2,1)S(1)}, u32[]{:S(2)}, u32[]{:S(2)}) collective-permute-start(bf16[16,256]{1,0:T(8,128)(2,1)S(1)} %get-tuple-element.63), channel_id=1, source_target_pairs={{0,2},{1,3},{2,0},{3,1},{4,6},{5,7},{6,4},{7,5},{8,10},{9,11},{10,... | collective-permute-start | bytes 24584 | tf_op jit(solution)/shard_map/dense_swap/ppermute | solution.py:456
  78.9 3.1 %collective-permute-start.3 = (bf16[16,256]{1,0:T(8,128)(2,1)S(1)}, bf16[16,256]{1,0:T(8,128)(2,1)S(1)}, u32[]{:S(2)}, u32[]{:S(2)}) collective-permute-start(bf16[16,256]{1,0:T(8,128)(2,1)S(1)} %get-tuple-element.64), channel_id=1, source_target_pairs={{0,3},{1,0},{2,1},{3,2},{4,7},{5,4},{6,5},{7,6},{8,11},{9,8},{10,9... | collective-permute-start | bytes 24584 | tf_op jit(solution)/shard_map/dense_swap/ppermute | solution.py:456
  82.0 0.0 collective-permute-done.1.dense1
  82.0 0.0 collective-permute-done.2.dense2
  82.0 1.6 %collective-permute-done.3.dense3 = bf16[16,256]{1,0:T(8,128)(2,1)S(1)} collective-permute-done((bf16[16,256]{1,0:T(8,128)(2,1)S(1)}, bf16[16,256]{1,0:T(8,128)(2,1)S(1)}, u32[]{:S(2)}, u32[]{:S(2)}) %collective-permute-start.3) | collective-permute-done | bytes 8224 | tf_op jit(solution)/shard_map/dense_swap/ppermute | solution.py:456
  83.6 4.2 %all-to-all-done.3 = bf16[512,2,128]{2,1,0:T(2,128)(2,1)S(1)} async-done(((bf16[512,2,128]{2,1,0:T(2,128)(2,1)}), bf16[512,2,128]{2,1,0:T(2,128)(2,1)S(1)}, u32[]{:S(2)}, u32[]{:S(2)}) %all-to-all-start.3) | async-done | bytes 262176 | tf_op jit(solution)/shard_map/all_to_all | solution.py:465
  87.8 0.8 final.1
Async XLA Ops:
  2.8 9.1 %all-to-all-start = ((bf16[4,16,256]{2,1,0:T(8,128)(2,1)}), bf16[4,16,256]{2,1,0:T(8,128)(2,1)S(1)}, u32[]{:S(2)}, u32[]{:S(2)}) async-start(bf16[4,16,256]{2,1,0:T(8,128)(2,1)} %spread.1), calls=%async_computation | async-start | bytes 65536 | tf_op jit(solution)/shard_map/gather/all_to_all | solution.py:357
  7.6 4.3 %copy-start.6 = (bf16[128,1024]{1,0:T(8,128)(2,1)S(1)}, bf16[128,1024]{1,0:T(8,128)(2,1)}, u32[]{:S(2)}) copy-start(bf16[128,1024]{1,0:T(8,128)(2,1)} %proj_out.1) | copy-start | bytes 786436
  22.3 2.3 %copy-start.7 = (bf16[1024]{0:T(1024)(128)(2,1)S(1)}, bf16[1024]{0:T(1024)(128)(2,1)}, u32[]{:S(2)}) copy-start(bf16[1024]{0:T(1024)(128)(2,1)} %ffn_gain.1) | copy-start | bytes 6148
  22.3 38.3 %collective-permute-start = (bf16[3072,128]{1,0:T(8,128)(2,1)S(1)}, bf16[3072,128]{1,0:T(8,128)(2,1)S(1)}, u32[]{:S(2)}, u32[]{:S(2)}) collective-permute-start(bf16[3072,128]{1,0:T(8,128)(2,1)S(1)} %get-tuple-element.58), channel_id=1, source_target_pairs={{0,1},{1,0},{2,3},{3,2},{4,5},{5,4},{6,7},{7,6},{8,9},{9,8},{10,11... | collective-permute-start | bytes 2359304 | tf_op jit(solution)/shard_map/swap/ppermute | solution.py:429
  24.6 36.0 %copy-start.2 = (bf16[1,128,1024]{2,1,0:T(8,128)(2,1)S(1)}, bf16[1,128,1024]{2,1,0:T(8,128)(2,1)}, u32[]{:S(2)}) copy-start(bf16[1,128,1024]{2,1,0:T(8,128)(2,1)} %param.53) | copy-start | bytes 786436
  25.0 35.6 %copy-start = (bf16[1,1024,128]{2,1,0:T(8,128)(2,1)S(1)}, bf16[1,1024,128]{2,1,0:T(8,128)(2,1)}, u32[]{:S(2)}) copy-start(bf16[1,1024,128]{2,1,0:T(8,128)(2,1)} %param.51) | copy-start | bytes 786436
  25.0 35.6 %copy-start.1 = (bf16[1,1024,128]{2,1,0:T(8,128)(2,1)S(1)}, bf16[1,1024,128]{2,1,0:T(8,128)(2,1)}, u32[]{:S(2)}) copy-start(bf16[1,1024,128]{2,1,0:T(8,128)(2,1)} %param.52) | copy-start | bytes 786436
  60.7 10.1 %copy-start.4 = (bf16[1024,256]{1,0:T(8,128)(2,1)S(1)}, bf16[1024,256]{1,0:T(8,128)(2,1)}, u32[]{:S(2)}) copy-start(bf16[1024,256]{1,0:T(8,128)(2,1)} %up.1) | copy-start | bytes 1572868
  60.7 10.1 %copy-start.5 = (bf16[1024,256]{1,0:T(8,128)(2,1)S(1)}, bf16[1024,256]{1,0:T(8,128)(2,1)}, u32[]{:S(2)}) copy-start(bf16[1024,256]{1,0:T(8,128)(2,1)} %down.1) | copy-start | bytes 1572868
  62.1 8.7 %copy-start.3 = (bf16[1024,256]{1,0:T(8,128)(2,1)S(1)}, bf16[1024,256]{1,0:T(8,128)(2,1)}, u32[]{:S(2)}) copy-start(bf16[1024,256]{1,0:T(8,128)(2,1)} %gate.1) | copy-start | bytes 1572868
  62.1 8.7 %copy-start.8 = (bf16[1024]{0:T(1024)(128)(2,1)S(1)}, bf16[1024]{0:T(1024)(128)(2,1)}, u32[]{:S(2)}) copy-start(bf16[1024]{0:T(1024)(128)(2,1)} %branch_gate.1) | copy-start | bytes 6148
  62.1 25.7 %all-to-all-start.3 = ((bf16[512,2,128]{2,1,0:T(2,128)(2,1)}), bf16[512,2,128]{2,1,0:T(2,128)(2,1)S(1)}, u32[]{:S(2)}, u32[]{:S(2)}) async-start(bf16[512,2,128]{2,1,0:T(2,128)(2,1)} %bitcast.15), calls=%async_computation.3 | async-start | bytes 524288 | tf_op jit(solution)/shard_map/all_to_all | solution.py:465
  71.2 10.7 %collective-permute-start.1 = (bf16[16,256]{1,0:T(8,128)(2,1)S(1)}, bf16[16,256]{1,0:T(8,128)(2,1)S(1)}, u32[]{:S(2)}, u32[]{:S(2)}) collective-permute-start(bf16[16,256]{1,0:T(8,128)(2,1)S(1)} %get-tuple-element.62), channel_id=1, source_target_pairs={{0,1},{1,2},{2,3},{3,0},{4,5},{5,6},{6,7},{7,4},{8,9},{9,10},{10,1... | collective-permute-start | bytes 24584 | tf_op jit(solution)/shard_map/dense_swap/ppermute | solution.py:456
  74.5 7.4 %collective-permute-start.2 = (bf16[16,256]{1,0:T(8,128)(2,1)S(1)}, bf16[16,256]{1,0:T(8,128)(2,1)S(1)}, u32[]{:S(2)}, u32[]{:S(2)}) collective-permute-start(bf16[16,256]{1,0:T(8,128)(2,1)S(1)} %get-tuple-element.63), channel_id=1, source_target_pairs={{0,2},{1,3},{2,0},{3,1},{4,6},{5,7},{6,4},{7,5},{8,10},{9,11},{10,... | collective-permute-start | bytes 24584 | tf_op jit(solution)/shard_map/dense_swap/ppermute | solution.py:456
  78.9 4.7 %collective-permute-start.3 = (bf16[16,256]{1,0:T(8,128)(2,1)S(1)}, bf16[16,256]{1,0:T(8,128)(2,1)S(1)}, u32[]{:S(2)}, u32[]{:S(2)}) collective-permute-start(bf16[16,256]{1,0:T(8,128)(2,1)S(1)} %get-tuple-element.64), channel_id=1, source_target_pairs={{0,3},{1,0},{2,1},{3,2},{4,7},{5,4},{6,5},{7,6},{8,11},{9,8},{10,9... | collective-permute-start | bytes 24584 | tf_op jit(solution)/shard_map/dense_swap/ppermute | solution.py:456

commit v2 on v1

--- a/solution.py
+++ b/solution.py
@@ -1,5 +1,3 @@
-import functools
-
 import jax
 import jax.numpy as jnp
 from jax import lax
@@ -7,6 +5,7 @@
 from jax.experimental.pallas import tpu as pltpu
 from jax.sharding import PartitionSpec as P
 
+
 HEADS = 8
 HEAD_DIM = 64
 STATE = 64
@@ -21,15 +20,16 @@
 LIMIT = 16 * 1024 * 1024
 
 
-def call(body, outs, specs, name, scratch=(), out_spec=VMEM):
+def call(body, outs, specs, scratch=(), out_spec=VMEM):
     return pl.pallas_call(
         body,
         out_shape=outs,
         in_specs=specs,
-        out_specs=jax.tree.map(lambda _: out_spec, outs),
+        out_specs=out_spec
+        if isinstance(out_spec, tuple)
+        else jax.tree.map(lambda _: out_spec, outs),
         scratch_shapes=scratch,
         compiler_params=pltpu.CompilerParams(vmem_limit_bytes=LIMIT),
-        name=name,
         interpret=INTERPRET,
     )
 
@@ -58,10 +58,11 @@
     return jnp.maximum(v, 0.0) + jnp.log1p(jnp.exp(-jnp.abs(v)))
 
 
-def spread_body(tokens, out, sems):
-    copies = [
-        pltpu.make_async_copy(tokens, out.at[j], sems.at[j]) for j in range(out.shape[0])
-    ]
+def spread_body(tokens, out, here, sems):
+    first = pltpu.make_async_copy(tokens, here, sems.at[out.shape[0]])
+    first.start()
+    first.wait()
+    copies = [pltpu.make_async_copy(here, out.at[j], sems.at[j]) for j in range(out.shape[0])]
     for copy in copies:
         copy.start()
     for copy in copies:
@@ -111,22 +112,32 @@
                     ] = kept
 
 
-STAGED = 14
+STAGED = 9
 
 
 def prepare_body(*refs):
     rank, ids, weights, bias, rate, skip, gate, up, down = refs[:9]
-    sources = refs[9 : 9 + STAGED]
-    select, combine, lanes, packed = refs[9 + STAGED : 13 + STAGED]
-    targets = refs[13 + STAGED : 13 + 2 * STAGED]
-    ids_here, weights_here, bias_here, rate_here, skip_here, sems = refs[13 + 2 * STAGED :]
+    proj_gate, proj_input, proj_write, proj_read, proj_step = refs[9:14]
+    sources = refs[14 : 14 + STAGED]
+    select, combine, lanes, packed, across, along = refs[14 + STAGED : 20 + STAGED]
+    targets = refs[20 + STAGED : 20 + 2 * STAGED]
+    ids_here, weights_here, bias_here, rate_here, skip_here, sems = refs[20 + 2 * STAGED :]
     width, block = gate.shape
+    inner = proj_gate.shape[1]
+    latent = proj_write.shape[0]
     pairs = [
         (ids, ids_here),
         (weights, weights_here),
         (bias, bias_here),
         (rate, rate_here),
         (skip, skip_here),
+    ]
+    pairs += [
+        (proj_gate, across.at[:, 0:inner]),
+        (proj_input, across.at[:, inner : 2 * inner]),
+        (proj_write, along.at[0:latent]),
+        (proj_read, along.at[latent : 2 * latent]),
+        (proj_step, along.at[2 * latent : 2 * latent + HEADS]),
     ]
     pairs += list(zip(sources, targets))
     pairs += [(gate, packed.at[0:width]), (up, packed.at[width : 2 * width])]
@@ -139,7 +150,6 @@
     for copy in copies[:5]:
         copy.wait()
     route(rank, ids_here, weights_here, select, combine)
-    inner = lanes.shape[1]
     heads = inner // HEAD_DIM
     lane_head = lax.broadcasted_iota(jnp.int32, (1, inner), 1) // HEAD_DIM
     for k, table in enumerate((bias_here, rate_here, skip_here)):
@@ -166,12 +176,9 @@
     rank,
     lanes,
     arrived,
+    across,
+    along,
     norm_gain,
-    proj_gate,
-    proj_input,
-    proj_write,
-    proj_read,
-    proj_step,
     taps_input,
     taps_write,
     taps_read,
@@ -191,15 +198,18 @@
     x = jnp.concatenate([arrived[j] for j in range(arrived.shape[0])], axis=1).astype(F32)
     scale = lax.rsqrt(jnp.mean(x * x, axis=-1, keepdims=True) + EPS)
     normed = (x * scale * norm_gain[...].astype(F32)[None, :]).astype(BF16)
-    gate_rows = nn(normed, proj_gate[...]).astype(BF16)
-    input_rows = nn(normed, proj_input[...]).astype(BF16)
-    write_rows = nt(normed, proj_write[...]).astype(BF16)
-    read_rows = nt(normed, proj_read[...]).astype(BF16)
-    step_all = nt(normed, proj_step[...])
+    inner = input_window.shape[2]
+    latent = write_window.shape[2]
+    first = nn(normed, across[...])
+    second = nt(normed, along[...])
+    gate_rows = first[:, 0:inner].astype(BF16)
+    input_rows = first[:, inner : 2 * inner].astype(BF16)
+    write_rows = second[:, 0:latent].astype(BF16)
+    read_rows = second[:, latent : 2 * latent].astype(BF16)
+    step_all = second[:, 2 * latent : 2 * latent + HEADS]
     input_conv = conv(input_window, input_rows, taps_input, new_input_window)
     write_conv = conv(write_window, write_rows, taps_write, new_write_window)
     read_conv = conv(read_window, read_rows, taps_read, new_read_window)
-    inner = input_conv.shape[1]
     heads = inner // HEAD_DIM
     lane_head = lax.broadcasted_iota(jnp.int32, (rows, inner), 1) // HEAD_DIM
     column = lax.broadcasted_iota(jnp.int32, step_all.shape, 1)
@@ -254,21 +264,26 @@
     hidden_part[...] = part.astype(BF16)
 
 
-def dense_body(
-    rank, normed_in, gate, up, down, branch_gate, out0, out1, out2, out3, branch, pieces
-):
+def dense_body(rank, normed_in, gate, up, down, branch_gate, give, keep, branch):
     normed = normed_in[...]
     hidden = (silu(nn(normed, gate[...])) * nn(normed, up[...])).astype(BF16)
     total = nt(hidden, down[...]).astype(BF16)
-    quarter = out0.shape[1]
-    for j in range(pieces.shape[0]):
-        pieces[j] = total[:, j * quarter : (j + 1) * quarter]
-    for k, out in enumerate((out0, out1, out2, out3)):
-        out[...] = pieces[jnp.bitwise_and(rank[0] + k, 3)]
+    half = give.shape[1]
+    upper = rank[0] > 1
+    give[...] = jnp.where(upper, total[:, 0:half], total[:, half:])
+    keep[...] = jnp.where(upper, total[:, half:], total[:, 0:half])
     level = jnp.sum(
         normed.astype(F32) * branch_gate[...].astype(F32)[None, :], axis=-1, keepdims=True
     )
     branch[...] = jnp.broadcast_to(jax.nn.sigmoid(level), branch.shape)
+
+
+def halve_body(rank, keep, got, give, left):
+    total = keep[...].astype(F32) + got[...].astype(F32)
+    quarter = give.shape[1]
+    odd = jnp.bitwise_and(rank[0], 1) > 0
+    give[...] = jnp.where(odd, total[:, 0:quarter], total[:, quarter:]).astype(BF16)
+    left[...] = jnp.where(odd, total[:, quarter:], total[:, 0:quarter])
 
 
 def expert_body(items, gate, up, down, other, out, unfolded, fold):
@@ -289,12 +304,10 @@
     out[...] = fold[...].astype(BF16)
 
 
-def final_body(returned, combine, dense0, dense1, dense2, dense3, branch, hidden_part, out):
+def final_body(returned, combine, left, got, branch, hidden_part, out):
     total = hidden_part[...].astype(F32)
     rows = total.shape[0]
-    dense = dense0[...].astype(F32)
-    for piece in (dense1, dense2, dense3):
-        dense += piece[...].astype(F32)
+    dense = left[...] + got[...].astype(F32)
     sums = nn(combine[...], returned[...])
     sums = sums[0 : 2 * rows] + sums[2 * rows :]
     total += jnp.concatenate([sums[0:rows], sums[rows:]], axis=1)
@@ -349,20 +362,14 @@
         spread_body,
         sds((tps, rows, quarter), BF16),
         [HBM],
-        "spread",
-        [pltpu.SemaphoreType.DMA((tps,))],
+        [pltpu.VMEM((rows, quarter), BF16), pltpu.SemaphoreType.DMA((tps + 1,))],
         HBM,
     )(kept(tokens))
-    with jax.named_scope("gather"):
-        arrived = lax.all_to_all(spread, "tp", 0, 0, tiled=True)
-
+    arrived = lax.all_to_all(spread, "tp", 0, 0, tiled=True)
+
+    projections = (proj_gate, proj_input, proj_write.T, proj_read.T, proj_step.T)
     staged = (
         norm_gain,
-        proj_gate,
-        proj_input,
-        proj_write.T,
-        proj_read.T,
-        proj_step.T,
         taps_input,
         taps_write,
         taps_read,
@@ -373,25 +380,27 @@
         out_gain,
     )
     ids, weights = expert_ids.T, expert_weights.T
-    select, combine, lanes, packed, *staged = call(
+    select, combine, *staged = call(
         prepare_body,
         (
-            sds((eps * pieces, rows * pieces), BF16),
-            sds((4 * rows, 2 * tps * eps), BF16),
-            sds((8, inner), F32),
-            sds((3 * width, block), BF16),
+            pltpu.VMEM((eps * pieces, rows * pieces), BF16),
+            pltpu.HBM((4 * rows, 2 * tps * eps), BF16),
+            pltpu.VMEM((8, inner), F32),
+            pltpu.HBM((3 * width, block), BF16),
+            pltpu.VMEM((width, 2 * inner), BF16),
+            pltpu.VMEM((2 * latent + HEADS, width), BF16),
         )
-        + tuple(sds(v.shape, v.dtype) for v in staged),
-        [SMEM] + [HBM] * (8 + STAGED),
-        "prepare",
+        + tuple(pltpu.VMEM(v.shape, v.dtype) for v in staged),
+        [SMEM] + [HBM] * (13 + STAGED),
         [
             pltpu.VMEM(ids.shape, ids.dtype),
             pltpu.VMEM(weights.shape, F32),
             pltpu.SMEM(step_bias.shape, F32),
             pltpu.SMEM(step_bias.shape, F32),
             pltpu.SMEM(step_bias.shape, F32),
-            pltpu.SemaphoreType.DMA((7 + pieces + STAGED,)),
+            pltpu.SemaphoreType.DMA((12 + pieces + STAGED,)),
         ],
+        (VMEM, VMEM, VMEM, HBM) + (VMEM,) * (2 + STAGED),
     )(
         rank,
         *map(
@@ -405,28 +414,27 @@
                 expert_gate[0],
                 expert_up[0],
                 expert_down[0],
+                *projections,
                 *staged,
             ),
         ),
     )
 
+    lanes, packed, *staged = staged
     partial, new_state, new_input, new_write, new_read = call(
         mixer_body,
         (
-            sds((tps, rows, width), BF16),
-            sds((rows, inner, STATE), F32),
-            sds((3, rows, inner), BF16),
-            sds((3, rows, latent), BF16),
-            sds((3, rows, latent), BF16),
+            pltpu.HBM((tps, rows, width), BF16),
+            pltpu.VMEM((rows, inner, STATE), F32),
+            pltpu.VMEM((3, rows, inner), BF16),
+            pltpu.VMEM((3, rows, latent), BF16),
+            pltpu.VMEM((3, rows, latent), BF16),
         ),
-        [SMEM] + [VMEM] * 17,
-        "mixer",
+        [SMEM] + [VMEM] * 14,
     )(rank, lanes, arrived, *staged, proj_out)
-    with jax.named_scope("mix"):
-        mixed_in = lax.all_to_all(partial, "tp", 0, 0, tiled=True)
-    packed, mixed_in = lax.optimization_barrier((packed, mixed_in))
-    with jax.named_scope("swap"):
-        other = lax.ppermute(packed, "tp", [(t, t ^ 1) for t in range(tps)])
+    mixed_in = lax.all_to_all(partial, "tp", 0, 0, tiled=True)
+    packed, _ = lax.optimization_barrier((packed, partial))
+    other = lax.ppermute(packed, "tp", [(t, t ^ 1) for t in range(tps)])
 
     outgoing, normed_ffn, hidden_part = call(
         hidden_body,
@@ -436,38 +444,33 @@
             sds((rows, quarter), BF16),
         ),
         [SMEM] + [VMEM] * 4,
-        "hidden",
         [pltpu.VMEM((rows * pieces, 128), F32)],
     )(rank, arrived, mixed_in, ffn_gain, select)
     items = lax.all_to_all(outgoing.reshape(eps, pieces, 128), "ep", 0, 0, tiled=True)
 
-    dense_out = call(
+    give, keep, branch = call(
         dense_body,
-        (sds((rows, quarter), BF16),) * tps + (sds((rows, 128), F32),),
+        (sds((rows, width // 2), BF16), sds((rows, width // 2), BF16), sds((rows, 128), F32)),
         [SMEM] + [VMEM] * 5,
-        "dense",
-        [pltpu.VMEM((tps, rows, quarter), BF16)],
     )(rank, normed_ffn, dense_gate, dense_up, dense_down, branch_gate)
-    branch = dense_out[tps]
-    dense_in = [dense_out[0]]
-    for k in range(1, tps):
-        with jax.named_scope("dense_swap"):
-            turn = [(t, (t + k) % tps) for t in range(tps)]
-            dense_in.append(lax.ppermute(dense_out[k], "tp", turn))
+    got = lax.ppermute(give, "tp", [(t, t ^ 2) for t in range(tps)])
+    give, left = call(
+        halve_body, (sds((rows, quarter), BF16), sds((rows, quarter), F32)), [SMEM] + [VMEM] * 2
+    )(rank, keep, got)
+    got = lax.ppermute(give, "tp", [(t, t ^ 1) for t in range(tps)])
 
     results = call(
         expert_body,
         sds((tps * eps * 2, 128), BF16),
         [VMEM] * 5,
-        "experts",
         [pltpu.VMEM((eps * pieces, 128), F32), pltpu.VMEM((tps * eps * 2, 128), F32)],
     )(items.reshape(eps * pieces, 128), expert_gate[0], expert_up[0], expert_down[0], other)
     returned = lax.all_to_all(
         results.reshape(tps * eps, 2, 128), ("tp", "ep"), 0, 0, tiled=True
     ).reshape(tps * eps * 2, 128)
 
-    new_hidden = call(final_body, sds((rows, quarter), BF16), [VMEM] * 8, "final")(
-        returned, combine, *dense_in, branch, hidden_part
+    new_hidden = call(final_body, sds((rows, quarter), BF16), [VMEM] * 6)(
+        returned, combine, left, got, branch, hidden_part
     )
     return (
         new_hidden,

time: 89 us -> 122 us (1.37)
  Pallas kernels: 10.2 us -> 33.2 us
  blocking collectives: 42.8 us -> 54.3 us
  local copies, waits for them, and re-layouts: 0.05 us -> 2.83 us
  waiting for transfers between devices: 8.13 us -> 5.61 us
  starting transfers between devices: 26.5 us -> 25 us
    pallas_call x6 -> x7, Pallas kernels: 9.9 us -> 32.9 us  [the longest x1 25.8 us: local(): call(prepare_body, (pltpu.VMEM((eps * pieces, rows * pieces), BF16), pltp...]
    all_to_all x1, blocking collectives: 7.2 us -> 15.6 us  [local(): mixed_in = lax.all_to_all(partial, 'tp', 0, 0, tiled=True)]
    all_to_all x1, blocking collectives: 35.6 us -> 38.8 us  [local(): lax.all_to_all(outgoing.reshape(eps, pieces, 128), 'ep', 0, 0, tiled=True)]
    unnamed x18 -> x26, local copies, waits for them, and re-layouts: 0.05 us -> 2.83 us
    ppermute x3 -> x2, starting transfers between devices: 10.7 us -> 8.15 us  [the longest x1 4.83 us: local(): got = lax.ppermute(give, 'tp', [(t, t ^ 2) for t in range(tps)])]
    all_to_all x1, waiting for transfers between devices: 2.32 us -> 0.01 us  [local(): arrived = lax.all_to_all(spread, 'tp', 0, 0, tiled=True)]
  transfers between devices with their start and end apart: 6 -> 5, of which waited for: 3 -> 2; matrix products, arithmetic and copies ran while one was open for 0% -> 2% of each run, Pallas kernels for 3% -> 22%
where the time goes in v2:
time: 122 us
  blocking collectives  54.3 us (45%)
  Pallas kernels  33.2 us (27%)
  starting transfers between devices  25 us (20%)
  waiting for transfers between devices  5.61 us (5%)
  local copies, waits for them, and re-layouts  2.83 us (2%)
    all_to_all x1, blocking collectives, local(): lax.all_to_all(outgoing.reshape(eps, pieces, 128), 'ep', 0, 0, tiled=True)  38.8 us
    pallas_call x1, Pallas kernels, local(): call(prepare_body, (pltpu.VMEM((eps * pieces, rows * pieces), BF16), pltp...  25.8 us
    all_to_all x1, blocking collectives, local(): mixed_in = lax.all_to_all(partial, 'tp', 0, 0, tiled=True)  15.6 us
    all_to_all x1, starting transfers between devices, local(): lax.all_to_all(results.reshape(tps * eps, 2, 128), ('tp', 'ep'), 0, 0, ti...  8.69 us
    all_to_all x1, starting transfers between devices, local(): arrived = lax.all_to_all(spread, 'tp', 0, 0, tiled=True)  4.84 us
    ppermute x1, starting transfers between devices, local(): got = lax.ppermute(give, 'tp', [(t, t ^ 2) for t in range(tps)])  4.83 us
    all_to_all x1, waiting for transfers between devices, local(): lax.all_to_all(results.reshape(tps * eps, 2, 128), ('tp', 'ep'), 0, 0, ti...  4.11 us
    ppermute x1, starting transfers between devices, local(): other = lax.ppermute(packed, 'tp', [(t, t ^ 1) for t in range(tps)])  3.36 us
  transfers between devices with their start and end apart: 5, of which 2 were waited for; matrix products, arithmetic and copies ran while one was open for 2% of the time, Pallas kernels for 22%

profile of v2, /device:TPU:1, one launch (start us, length us, event | category | flops | bytes accessed | tf_op | source)
XLA Modules:
  0.0 121.9 jit_solution(15265898596845184217)
XLA Ops:
  0.6 1.3 %shard_map.308 = bf16[4,16,256]{2,1,0:T(8,128)(2,1)} custom-call(bf16[16,256]{1,0:T(8,128)(2,1)} %tokens.1), custom_call_target="tpu_custom_call" | custom-call | tf_op jit(solution)/shard_map/pallas_call | solution.py:361
  2.0 4.8 %all-to-all-start = ((bf16[4,16,256]{2,1,0:T(8,128)(2,1)}), bf16[4,16,256]{2,1,0:T(8,128)(2,1)S(1)}, u32[]{:S(2)}, u32[]{:S(2)}) async-start(bf16[4,16,256]{2,1,0:T(8,128)(2,1)} %shard_map.308), calls=%async_computation | async-start | bytes 65536 | tf_op jit(solution)/shard_map/all_to_all | solution.py:368
  6.8 0.0 copy-start.6
  6.8 25.8 %shard_map.309 = (bf16[1024,128]{1,0:T(8,128)(2,1)S(1)}, bf16[64,1024]{1,0:T(8,128)(2,1)}, f32[8,128]{1,0:T(8,128)S(1)}, bf16[3072,128]{1,0:T(8,128)(2,1)}, bf16...) custom-call(s32[1]{0:T(128)} %bitcast.refs_0_.rank, ...), custom_call_target="tpu_custom_call" | custom-call | tf_op jit(solution)/shard_map/pallas_call | solution.py:383
  32.7 0.0 all-to-all-done.arrived
  32.7 0.0 copy-done.6
  32.7 0.0 copy-start.10
  32.7 3.1 %shard_map.310 = (bf16[4,16,1024]{2,1,0:T(8,128)(2,1)}, f32[16,128,64]{2,1,0:T(8,128)S(1)}, bf16[3,16,128]{2,1,0:T(8,128)(2,1)S(1)}, bf16[3,16,64]{2,1,0:T(8,128)(2,1)S(1)}, bf16[3,16,64]{2,1,0:T(8,128)(2,1)S(1)}) custom-call(s32[1]{0:T(128)} %bitcast.refs_0_.rank, f32[8,128]{1,0:T(8,128)S(1)} %get-tuple-element.34.lanes, ...), custom_call_target="tpu_custom_call" | custom-call | tf_op jit(solution)/shard_map/pallas_call | solution.py:424
  35.8 0.0 copy-done.10
  35.8 3.4 %collective-permute-start = (bf16[3072,128]{1,0:T(8,128)(2,1)S(1)}, bf16[3072,128]{1,0:T(8,128)(2,1)S(1)}, u32[]{:S(2)}, u32[]{:S(2)}) collective-permute-start(bf16[3072,128]{1,0:T(8,128)(2,1)S(1)} %copy-done.10), channel_id=1, source_target_pairs={{0,1},{1,0},{2,3},{3,2},{4,5},{5,4},{6,7},{7,6},{8,9},{9,8},{10,11... | collective-permute-start | bytes 2359304 | tf_op jit(solution)/shard_map/ppermute | solution.py:437
  39.2 0.0 copy-start.8
  39.2 15.6 %all_to_all.20.mixed_in = bf16[4,16,1024]{2,1,0:T(8,128)(2,1)S(1)} all-to-all(bf16[4,16,1024]{2,1,0:T(8,128)(2,1)} %get-tuple-element.46), channel_id=1, replica_groups=mesh['ep'=128,'tp'=4] {'tp'}, dimensions={0} | all-to-all | bytes 262144 | tf_op jit(solution)/shard_map/all_to_all | solution.py:435
  54.8 0.0 copy-done.8
  54.8 0.0 copy-start.2
  54.8 0.3 shard_map.311
  55.1 0.0 copy-start
  55.1 0.0 copy-start.1
  55.1 38.8 %all_to_all.21 = bf16[128,8,128]{2,1,0:T(8,128)(2,1)S(1)} all-to-all(bf16[128,8,128]{2,1,0:T(8,128)(2,1)S(1)} %bitcast.33), channel_id=1, replica_groups=mesh['ep'=128,'tp'=4] {'ep'}, dimensions={0} | all-to-all | bytes 524288 | tf_op jit(solution)/shard_map/all_to_all | solution.py:449
  93.9 0.0 collective-permute-done.other
  93.9 0.0 copy-done.2
  93.9 0.0 copy-done
  93.9 0.0 copy-done.1
  93.9 0.0 copy-start.4
  93.9 0.0 copy-start.5
  93.9 1.4 %shard_map.312 = bf16[1024,128]{1,0:T(8,128)(2,1)} custom-call(bf16[1024,128]{1,0:T(8,128)(2,1)S(1)} %bitcast.32, bf16[1024,128]{1,0:T(8,128)(2,1)S(1)} %bitcast.27, bf16[1024,128]{1,0:T(8,128)(2,1)S(1)} %bitcast.29, bf16[128,1024]{1,0:T(8,128)(2,1)S(1)} %bitcast.31, bf16[3072,128]{1,0:T(8,128)(2,1)S(1)} %collective-permute-done.other), custom_call_target="tpu_custom_call" | custom-call | tf_op jit(solution)/shard_map/pallas_call | solution.py:462
  95.4 0.0 copy-start.3
  95.4 0.0 copy-start.9
  95.4 8.7 %all-to-all-start.3 = ((bf16[512,2,128]{2,1,0:T(2,128)(2,1)}), bf16[512,2,128]{2,1,0:T(2,128)(2,1)S(1)}, u32[]{:S(2)}, u32[]{:S(2)}) async-start(bf16[512,2,128]{2,1,0:T(2,128)(2,1)} %bitcast.15), calls=%async_computation.3 | async-start | bytes 524288 | tf_op jit(solution)/shard_map/all_to_all | solution.py:468
  104.1 0.0 copy-done.4
  104.1 0.0 copy-done.5
  104.1 0.0 copy-done.3
  104.1 0.0 copy-done.9
  104.1 0.4 shard_map.313
  104.5 4.8 %collective-permute-start.1 = (bf16[16,512]{1,0:T(8,128)(2,1)S(1)}, bf16[16,512]{1,0:T(8,128)(2,1)S(1)}, u32[]{:S(2)}, u32[]{:S(2)}) collective-permute-start(bf16[16,512]{1,0:T(8,128)(2,1)S(1)} %get-tuple-element.54), channel_id=1, source_target_pairs={{0,2},{1,3},{2,0},{3,1},{4,6},{5,7},{6,4},{7,5},{8,10},{9,11},{10,... | collective-permute-start | bytes 49160 | tf_op jit(solution)/shard_map/ppermute | solution.py:456
  109.4 1.5 %collective-permute-done.1.got = bf16[16,512]{1,0:T(8,128)(2,1)S(1)} collective-permute-done((bf16[16,512]{1,0:T(8,128)(2,1)S(1)}, bf16[16,512]{1,0:T(8,128)(2,1)S(1)}, u32[]{:S(2)}, u32[]{:S(2)}) %collective-permute-start.1) | collective-permute-done | bytes 16416 | tf_op jit(solution)/shard_map/ppermute | solution.py:456
  110.9 3.3 %collective-permute-start.2 = (bf16[16,256]{1,0:T(8,128)(2,1)S(1)}, bf16[16,256]{1,0:T(8,128)(2,1)S(1)}, u32[]{:S(2)}, u32[]{:S(2)}) collective-permute-start(bf16[16,256]{1,0:T(8,128)(2,1)S(1)} %get-tuple-element.56), channel_id=1, source_target_pairs={{0,1},{1,0},{2,3},{3,2},{4,5},{5,4},{6,7},{7,6},{8,9},{9,8},{10,11... | collective-permute-start | bytes 24584 | tf_op jit(solution)/shard_map/ppermute | solution.py:460
  114.2 0.0 copy-start.7
  114.2 1.0 copy.34
  115.2 0.6 copy.35
  115.8 0.6 copy.36
  116.4 0.6 copy.37
  117.0 0.0 collective-permute-done.2.got
  117.0 4.1 %all-to-all-done.3 = bf16[512,2,128]{2,1,0:T(2,128)(2,1)S(1)} async-done(((bf16[512,2,128]{2,1,0:T(2,128)(2,1)}), bf16[512,2,128]{2,1,0:T(2,128)(2,1)S(1)}, u32[]{:S(2)}, u32[]{:S(2)}) %all-to-all-start.3) | async-done | bytes 262176 | tf_op jit(solution)/shard_map/all_to_all | solution.py:468
  121.1 0.0 copy-done.7
  121.1 0.8 shard_map.315
  (1 shorter events, 0.0 us)
Async XLA Ops:
  2.0 30.7 %all-to-all-start = ((bf16[4,16,256]{2,1,0:T(8,128)(2,1)}), bf16[4,16,256]{2,1,0:T(8,128)(2,1)S(1)}, u32[]{:S(2)}, u32[]{:S(2)}) async-start(bf16[4,16,256]{2,1,0:T(8,128)(2,1)} %shard_map.308), calls=%async_computation | async-start | bytes 65536 | tf_op jit(solution)/shard_map/all_to_all | solution.py:368
  6.8 25.9 %copy-start.6 = (bf16[128,1024]{1,0:T(8,128)(2,1)S(1)}, bf16[128,1024]{1,0:T(8,128)(2,1)}, u32[]{:S(2)}) copy-start(bf16[128,1024]{1,0:T(8,128)(2,1)} %proj_out.1) | copy-start | bytes 786436
  32.7 3.1 %copy-start.10 = (bf16[3072,128]{1,0:T(8,128)(2,1)S(1)}, bf16[3072,128]{1,0:T(8,128)(2,1)}, u32[]{:S(2)}) copy-start(bf16[3072,128]{1,0:T(8,128)(2,1)} %get-tuple-element.50) | copy-start | bytes 2359300
  35.8 58.1 %collective-permute-start = (bf16[3072,128]{1,0:T(8,128)(2,1)S(1)}, bf16[3072,128]{1,0:T(8,128)(2,1)S(1)}, u32[]{:S(2)}, u32[]{:S(2)}) collective-permute-start(bf16[3072,128]{1,0:T(8,128)(2,1)S(1)} %copy-done.10), channel_id=1, source_target_pairs={{0,1},{1,0},{2,3},{3,2},{4,5},{5,4},{6,7},{7,6},{8,9},{9,8},{10,11... | collective-permute-start | bytes 2359304 | tf_op jit(solution)/shard_map/ppermute | solution.py:437
  39.2 15.6 %copy-start.8 = (bf16[1024]{0:T(1024)(128)(2,1)S(1)}, bf16[1024]{0:T(1024)(128)(2,1)}, u32[]{:S(2)}) copy-start(bf16[1024]{0:T(1024)(128)(2,1)} %ffn_gain.1) | copy-start | bytes 6148
  54.8 39.1 %copy-start.2 = (bf16[1,128,1024]{2,1,0:T(8,128)(2,1)S(1)}, bf16[1,128,1024]{2,1,0:T(8,128)(2,1)}, u32[]{:S(2)}) copy-start(bf16[1,128,1024]{2,1,0:T(8,128)(2,1)} %param.53) | copy-start | bytes 786436
  55.1 38.8 %copy-start = (bf16[1,1024,128]{2,1,0:T(8,128)(2,1)S(1)}, bf16[1,1024,128]{2,1,0:T(8,128)(2,1)}, u32[]{:S(2)}) copy-start(bf16[1,1024,128]{2,1,0:T(8,128)(2,1)} %param.51) | copy-start | bytes 786436
  55.1 38.8 %copy-start.1 = (bf16[1,1024,128]{2,1,0:T(8,128)(2,1)S(1)}, bf16[1,1024,128]{2,1,0:T(8,128)(2,1)}, u32[]{:S(2)}) copy-start(bf16[1,1024,128]{2,1,0:T(8,128)(2,1)} %param.52) | copy-start | bytes 786436
  93.9 10.1 %copy-start.4 = (bf16[1024,256]{1,0:T(8,128)(2,1)S(1)}, bf16[1024,256]{1,0:T(8,128)(2,1)}, u32[]{:S(2)}) copy-start(bf16[1024,256]{1,0:T(8,128)(2,1)} %up.1) | copy-start | bytes 1572868
  93.9 10.1 %copy-start.5 = (bf16[1024,256]{1,0:T(8,128)(2,1)S(1)}, bf16[1024,256]{1,0:T(8,128)(2,1)}, u32[]{:S(2)}) copy-start(bf16[1024,256]{1,0:T(8,128)(2,1)} %down.1) | copy-start | bytes 1572868
  95.4 8.7 %copy-start.3 = (bf16[1024,256]{1,0:T(8,128)(2,1)S(1)}, bf16[1024,256]{1,0:T(8,128)(2,1)}, u32[]{:S(2)}) copy-start(bf16[1024,256]{1,0:T(8,128)(2,1)} %gate.1) | copy-start | bytes 1572868
  95.4 8.7 %copy-start.9 = (bf16[1024]{0:T(1024)(128)(2,1)S(1)}, bf16[1024]{0:T(1024)(128)(2,1)}, u32[]{:S(2)}) copy-start(bf16[1024]{0:T(1024)(128)(2,1)} %branch_gate.1) | copy-start | bytes 6148
  95.4 25.7 %all-to-all-start.3 = ((bf16[512,2,128]{2,1,0:T(2,128)(2,1)}), bf16[512,2,128]{2,1,0:T(2,128)(2,1)S(1)}, u32[]{:S(2)}, u32[]{:S(2)}) async-start(bf16[512,2,128]{2,1,0:T(2,128)(2,1)} %bitcast.15), calls=%async_computation.3 | async-start | bytes 524288 | tf_op jit(solution)/shard_map/all_to_all | solution.py:468
  104.5 6.3 %collective-permute-start.1 = (bf16[16,512]{1,0:T(8,128)(2,1)S(1)}, bf16[16,512]{1,0:T(8,128)(2,1)S(1)}, u32[]{:S(2)}, u32[]{:S(2)}) collective-permute-start(bf16[16,512]{1,0:T(8,128)(2,1)S(1)} %get-tuple-element.54), channel_id=1, source_target_pairs={{0,2},{1,3},{2,0},{3,1},{4,6},{5,7},{6,4},{7,5},{8,10},{9,11},{10,... | collective-permute-start | bytes 49160 | tf_op jit(solution)/shard_map/ppermute | solution.py:456
  110.9 6.1 %collective-permute-start.2 = (bf16[16,256]{1,0:T(8,128)(2,1)S(1)}, bf16[16,256]{1,0:T(8,128)(2,1)S(1)}, u32[]{:S(2)}, u32[]{:S(2)}) collective-permute-start(bf16[16,256]{1,0:T(8,128)(2,1)S(1)} %get-tuple-element.56), channel_id=1, source_target_pairs={{0,1},{1,0},{2,3},{3,2},{4,5},{5,4},{6,7},{7,6},{8,9},{9,8},{10,11... | collective-permute-start | bytes 24584 | tf_op jit(solution)/shard_map/ppermute | solution.py:460
  114.2 6.9 %copy-start.7 = (bf16[64,1024]{1,0:T(8,128)(2,1)S(1)}, bf16[64,1024]{1,0:T(8,128)(2,1)}, u32[]{:S(2)}) copy-start(bf16[64,1024]{1,0:T(8,128)(2,1)} %get-tuple-element.51.combine) | copy-start | bytes 393220
